TPU v7x, 512 devices: a whole 4x4x16 slice. The times are simulated.
512 devices in a mesh: ep: 32 (over z, core), tp: 16 (over y, x).
Axes of the slice: x: 4, y: 4, z: 16, core: 2. Of those that a mesh axis runs over, the one named last changes fastest.
Arguments:
- probe_preactivations: bfloat16 [16384, 2048], P('ep', 'tp'), may hold values from -6 to 6
- rightward_retain_scores: bfloat16 [16384, 2048], P('ep', 'tp'), may hold values from -5.5 to 5.5
- leftward_retain_scores: bfloat16 [16384, 2048], P('ep', 'tp'), may hold values from -5.5 to 5.5
- payload_vectors: bfloat16 [16384, 2048], P('ep', 'tp'), may hold values from -6 to 6
- retain_minimum_bounds: float32 [2, 2048], P(None, 'tp'), may hold values from 0.88 to 1
- extra_shrink_spikes: float32 [16, 16384], P('tp', 'ep'), may hold values from -0.7 to 0
- mixer_rescale_factor: float32 [2048], P('tp'), may hold values from 0.1 to 1.9
- mixer_emit_matrix: bfloat16 [2048, 2048], P('tp'), may hold values from -0.1875 to 0.1875
- specialist_arriving_tokens: bfloat16 [4096, 2048], P('ep'), may hold values from -6 to 6
- specialist_rescale_factor: float32 [2048], replicated, may hold values from 0.1 to 1.9
- routed_specialist_ids: int32 [4096, 2], P('ep'), may hold values from 0 to 31, all different within a row; in each aligned block of 128 rows (0 to 127, 128 to 255, ...) at most 16 rows name the same one
- routed_specialist_shares: float32 [4096, 2], P('ep'), may hold values from 0.1 to 1
- specialist_switch_matrix: bfloat16 [32, 2048, 3584], P('ep', None, 'tp'), may hold values from -0.125 to 0.125
- specialist_widen_matrix: bfloat16 [32, 2048, 3584], P('ep', None, 'tp'), may hold values from -0.125 to 0.125
- specialist_shrink_matrix: bfloat16 [32, 3584, 2048], P('ep', 'tp'), may hold values from -0.125 to 0.125
Outputs:
- mixed_a: bfloat16 [16384, 2048], P('ep', 'tp')
- mixed_b: bfloat16 [4096, 2048], P('ep', 'tp')
Inputs may be any that keep to these rules, and one draw needn't show every extreme that they name: `routed_specialist_ids`: each row names 2 different experts; within the rows of one index of ep no expert is named by more than 16 rows, and in every draw some expert is named by exactly 16 rows of some index.
All inputs are finite; a program needn't handle non-finite values.
Results may differ from a plain program's by a relative error of at most 0.015.
Values may be sent and summed in bfloat16 or wider, within the bound.
A program may use at most 64 MiB of HBM per device.

v0:
```python
import jax
import jax.numpy as jnp
from jax import lax
from jax.sharding import Mesh
from jax.sharding import PartitionSpec as P

D = 2048
DK = 128
SPAN = 32
EP = ("ep_0", "ep_1")


EPS = 1e-06
NEG_BIG = -1e30


def filled_with(shard, identity):
    return jax.tree.map(
        lambda a, e: jnp.broadcast_to(jnp.asarray(e, a.dtype), a.shape), shard, identity
    )


def collected_together(shard, axis):
    leaves = jax.tree.leaves(shard)
    turns = sorted(range(len(leaves)), key=lambda k: -leaves[k].size)
    width = (1, *leaves[turns[0]].shape)[-1]
    lines = [
        jnp.pad(leaves[k].reshape(-1), (0, -leaves[k].size % width)).reshape(-1, width)
        for k in turns
    ]
    both, at, found = (lax.all_gather(jnp.concatenate(lines), axis), 0, {})
    for k, line in zip(turns, lines):
        share = both[:, at : at + len(line)].reshape(len(both), -1)
        found[k] = share[:, : leaves[k].size].reshape(-1, *leaves[k].shape)
        at += len(line)
    numbers = iter(range(len(leaves)))
    return jax.tree.map(lambda _: found[next(numbers)], shard)


def entering(shard, axes, combine, identity, reverse):
    before = start = filled_with(shard, identity)
    so_far = shard
    for axis in reversed(axes):
        peers, position = (lax.axis_size(axis), lax.axis_index(axis))
        pieces = collected_together(
            jax.tree.map(
                lambda part, kind: part.astype(kind), so_far, (jnp.bfloat16, jnp.bfloat16)
            ),
            axis,
        )
        inside, so_far = (start, start)
        for k in reversed(range(peers)) if reverse else range(peers):
            passed = k > position if reverse else k < position
            so_far = combine(
                so_far, jax.tree.map(lambda part, own: part[k].astype(own.dtype), pieces, shard)
            )
            inside = jax.tree.map(lambda new, old: jnp.where(passed, new, old), so_far, inside)
        before = combine(inside, before)
    return before


def from_everyone(shard, axis):
    peers = lax.axis_size(axis)
    return lax.all_to_all(
        jnp.broadcast_to(shard[None], (peers, *shard.shape)), axis, 0, 0, tiled=True
    )


def laid_out(blocks, dim):
    blocks = jnp.moveaxis(blocks, 0, dim)
    dims = blocks.shape
    return blocks.reshape(*dims[:dim], dims[dim] * dims[dim + 1], *dims[dim + 2 :])


def gather_directly(shard, axis, dim):
    blocks = from_everyone(shard, axis)
    return laid_out(blocks, dim)


def cut_along(shard, dim, peers):
    dims = shard.shape
    blocks = shard.reshape(*dims[:dim], peers, dims[dim] // peers, *dims[dim + 1 :])
    return jnp.moveaxis(blocks, dim, 0)


def summed_on_arrival(shard, axis, dim):
    blocks = cut_along(shard, dim, lax.axis_size(axis))
    arrived = lax.all_to_all(blocks, axis, split_axis=0, concat_axis=0, tiled=True)
    return arrived.astype(jnp.float32).sum(axis=0)


def recurrence(query_heads, key_gate, v_heads, shrink_exponent, state_in):
    channel_group_count, length, _ = query_heads.shape
    block_count = length // SPAN

    def blocks(tensor):
        return jnp.moveaxis(
            tensor.reshape(channel_group_count, block_count, SPAN, tensor.shape[-1]), 1, 0
        )

    lower_tri = jnp.tril(jnp.ones((SPAN, SPAN), dtype=bool))[:, :, None]

    def advance(carried_state, pieces):
        query_block, key_block, value_block, l_blk = pieces
        cumulative_decay = jnp.cumsum(l_blk, axis=1)
        block_final_state = cumulative_decay[:, -1:, :]
        relative = cumulative_decay[:, :, None, :] - cumulative_decay[:, None, :, :]
        decays = jnp.exp(jnp.where(lower_tri, relative, NEG_BIG))
        scores = jnp.einsum("htk,hsk,htsk->hts", query_block, key_block, decays)
        block_result = jnp.einsum("hts,hsv->htv", scores, value_block)
        block_result = block_result + jnp.einsum(
            "dyr,dru->dyu", query_block * jnp.exp(cumulative_decay), carried_state
        )
        carried_state = jnp.exp(block_final_state[:, 0, :])[
            :, :, None
        ] * carried_state + jnp.einsum(
            "qfw,qfa->qwa", key_block * jnp.exp(block_final_state - cumulative_decay), value_block
        )
        return (carried_state, block_result)

    final_state, block_outs = lax.scan(
        advance,
        state_in,
        (blocks(query_heads), blocks(key_gate), blocks(v_heads), blocks(shrink_exponent)),
    )
    return (
        jnp.moveaxis(block_outs, 0, 1).reshape(channel_group_count, length, v_heads.shape[-1]),
        final_state,
    )


def to_heads(matrix, channel_group_count):
    length = matrix.shape[0]
    return matrix.astype(jnp.float32).reshape(length, channel_group_count, -1).transpose(1, 0, 2)


def retain_factors(retain_scores, retain_minimum, extra_shrink_spikes, channel_group_count):
    pre_act = to_heads(retain_scores, channel_group_count)
    floor_b = retain_minimum.reshape(channel_group_count, 1, -1)
    retain_factor = floor_b + (1.0 - floor_b) * jax.nn.sigmoid(pre_act)
    shrink_exponent = jnp.log(retain_factor) + extra_shrink_spikes[:, :, None]
    key_gate = (1.0 - floor_b) * jax.nn.sigmoid(-pre_act)
    return (key_gate, shrink_exponent)


def reverse_seq(tensor):
    return jnp.flip(tensor, axis=1)


def chain_join(earlier, later_part):
    decay_a, state_a = earlier
    decay_b, state_b = later_part
    return (decay_a + decay_b, jnp.exp(decay_b)[:, :, None] * state_a + state_b)


def rounded(partial_value):
    return lax.optimization_barrier(partial_value.astype(jnp.bfloat16)).astype(jnp.float32)


def expert_hidden(slot_block, gate_w, up_w):
    gate_out = jnp.einsum("scd,df->scf", slot_block, gate_w, preferred_element_type=jnp.float32)
    up_out = jnp.einsum("scd,df->scf", slot_block, up_w, preferred_element_type=jnp.float32)
    return (jax.nn.silu(gate_out) * up_out).astype(jnp.bfloat16)


def per_device(
    probe_preactivations,
    rightward_retain_scores,
    leftward_retain_scores,
    payload_vectors,
    retain_minimum_bounds,
    extra_shrink_spikes,
    mixer_rescale_factor,
    mixer_emit_matrix,
    specialist_arriving_tokens,
    specialist_rescale_factor,
    routed_specialist_ids,
    routed_specialist_shares,
    specialist_switch_matrix,
    specialist_widen_matrix,
    specialist_shrink_matrix,
):
    ep_count = lax.axis_size(EP)
    tp_count = lax.axis_size("tp")
    local_channel_groups = probe_preactivations.shape[1] // DK
    tok_local = probe_preactivations.shape[0]
    query_heads = jax.nn.silu(to_heads(probe_preactivations, local_channel_groups))
    v_heads = to_heads(payload_vectors, local_channel_groups)
    value_width = v_heads.shape[-1]
    rightward_seed, rightward_shrink_exponent = retain_factors(
        rightward_retain_scores, retain_minimum_bounds[0], extra_shrink_spikes, local_channel_groups
    )
    leftward_seed, leftward_shrink_exponent = retain_factors(
        leftward_retain_scores, retain_minimum_bounds[1], extra_shrink_spikes, local_channel_groups
    )
    zero_state = jnp.zeros((local_channel_groups, DK, value_width), jnp.float32)
    zero_decay = jnp.zeros((local_channel_groups, DK), jnp.float32)
    out_fwd, end_fwd = recurrence(
        query_heads, rightward_seed, v_heads, rightward_shrink_exponent, zero_state
    )
    _, forward_entry_state = entering(
        (jnp.sum(rightward_shrink_exponent, axis=1), end_fwd),
        EP,
        chain_join,
        (zero_decay, zero_state),
        False,
    )
    out_fwd = out_fwd + jnp.einsum(
        "dyr,dru->dyu",
        query_heads * jnp.exp(jnp.cumsum(rightward_shrink_exponent, axis=1)),
        forward_entry_state,
    )
    reversed_query = reverse_seq(query_heads)
    reversed_log_decay = reverse_seq(leftward_shrink_exponent)
    out_rev, end_rev = recurrence(
        reversed_query,
        reverse_seq(leftward_seed),
        reverse_seq(v_heads),
        reversed_log_decay,
        zero_state,
    )
    _, reverse_entry_state = entering(
        (jnp.sum(reversed_log_decay, axis=1), end_rev),
        EP,
        chain_join,
        (zero_decay, zero_state),
        True,
    )
    out_rev = out_rev + jnp.einsum(
        "dyr,dru->dyu",
        reversed_query * jnp.exp(jnp.cumsum(reversed_log_decay, axis=1)),
        reverse_entry_state,
    )
    combined = out_fwd + reverse_seq(out_rev)
    normed = combined * lax.rsqrt(jnp.mean(combined * combined, axis=-1, keepdims=True) + EPS)
    normed = normed * mixer_rescale_factor.reshape(local_channel_groups, 1, value_width)
    mixed_heads = normed.transpose(1, 0, 2).reshape(tok_local, -1).astype(jnp.bfloat16)
    rows_b = specialist_arriving_tokens.shape[0]
    top_count = routed_specialist_ids.shape[1]
    capacity = 2 * rows_b * top_count // ep_count
    rows_f = specialist_arriving_tokens.astype(jnp.float32)
    normed_b = (
        rows_f
        * lax.rsqrt(jnp.mean(rows_f * rows_f, axis=-1, keepdims=True) + EPS)
        * specialist_rescale_factor
    ).astype(jnp.bfloat16)
    flat_ids = routed_specialist_ids.reshape(-1)
    onehot = (flat_ids[:, None] == jnp.arange(ep_count, dtype=jnp.int32)[None, :]).astype(jnp.int32)
    ranking = jnp.sum((jnp.cumsum(onehot, axis=0) - onehot) * onehot, axis=1)
    slot_of = flat_ids * capacity + ranking
    slot_grid = jnp.arange(ep_count * capacity, dtype=jnp.int32)
    matches = slot_grid[:, None] == slot_of[None, :]
    copy_row = jnp.arange(rows_b * top_count, dtype=jnp.int32) // top_count
    source_row = jnp.sum(jnp.where(matches, copy_row[None, :], 0), axis=1).reshape(
        ep_count, capacity
    )
    occupied = jnp.any(matches, axis=1).reshape(ep_count, capacity).astype(jnp.bfloat16)
    per_part = capacity // tp_count
    offset = lax.axis_index("tp") * per_part
    part_rows = lax.dynamic_slice_in_dim(source_row, offset, per_part, 1)
    part_live = lax.dynamic_slice_in_dim(occupied, offset, per_part, 1)
    outgoing = normed_b[part_rows] * part_live[:, :, None]
    arrived = lax.all_to_all(outgoing, EP, split_axis=0, concat_axis=0, tiled=True)
    hidden = expert_hidden(
        gather_directly(arrived, "tp", 1), specialist_switch_matrix[0], specialist_widen_matrix[0]
    )
    hidden = hidden.reshape(-1, hidden.shape[-1])
    share_cols = D // tp_count
    columns = mixer_emit_matrix
    partial_value = lax.dot_general(
        columns, mixed_heads, (((0,), (1,)), ((), ())), preferred_element_type=jnp.float32
    )
    columns = specialist_shrink_matrix[0]
    expert_partial_value = lax.dot_general(
        columns, hidden, (((0,), (1,)), ((), ())), preferred_element_type=jnp.float32
    )
    summed = summed_on_arrival(
        jnp.concatenate([rounded(partial_value), rounded(expert_partial_value)], axis=1).astype(
            jnp.bfloat16
        ),
        "tp",
        0,
    )
    mixer_total = summed[:, :tok_local]
    expert_total = summed[:, tok_local:]
    mixed_a = mixer_total.astype(jnp.bfloat16).T
    outgoing_back = expert_total.astype(jnp.bfloat16).T.reshape(ep_count, capacity, share_cols)
    returned = lax.all_to_all(outgoing_back, EP, split_axis=0, concat_axis=0, tiled=True)
    copies = returned.reshape(ep_count * capacity, share_cols)[slot_of].astype(jnp.float32)
    copies = copies.reshape(rows_b, top_count, share_cols)
    mixed_b = jnp.sum(copies * routed_specialist_shares[:, :, None], axis=1).astype(jnp.bfloat16)
    return (mixed_a, mixed_b)


def solution(mesh):
    split = Mesh(mesh.devices.reshape(16, 2, mesh.shape["tp"]), ("ep_0", "ep_1", "tp"))
    return jax.shard_map(
        per_device,
        mesh=split,
        in_specs=(
            P(EP, "tp"),
            P(EP, "tp"),
            P(EP, "tp"),
            P(EP, "tp"),
            P(None, "tp"),
            P("tp", EP),
            P("tp"),
            P("tp", None),
            P(EP, None),
            P(),
            P(EP, None),
            P(EP, None),
            P(EP, None, "tp"),
            P(EP, None, "tp"),
            P(EP, "tp", None),
        ),
        out_specs=(P(EP, "tp"), P(EP, "tp")),
        check_vma=False,
    )
```

profile of v0, /device:TPU:1, one launch (start us, length us, event | category | flops | bytes accessed | tf_op | source)
XLA Modules:
  0.0 242.3 jit_solution(15821496324138785126)
XLA Ops:
  0.6 0.9 copy.184
  1.8 0.6 reduce-window.26
  3.4 1.2 fusion.75
  4.9 1.2 fusion.77
  6.2 0.7 gather_fusion
  6.9 0.5 broadcast.676
  7.4 0.7 reduce.18
  8.1 0.7 reshape.1893
  8.8 16.7 %all-to-all-start = ((bf16[32,2,1024]{2,1,0:T(2,128)(2,1)}), bf16[32,2,1024]{2,1,0:T(2,128)(2,1)S(1)}, u32[]{:S(2)}, u32[]{:S(2)}) async-start(bf16[32,2,1024]{2,1,0:T(2,128)(2,1)} %reshape.1893), calls=%async_computation | async-start | bytes 262144 | tf_op jit(solution)/shard_map/all_to_all | solution.py:263
  25.7 0.4 fusion.104
  26.8 20.0 %while.27 = (s32[]{:T(128)}, f32[1,128,128]{2,1,0:T(8,128)S(1)}, f32[16,1,32,128]{3,2,1,0:T(8,128)S(1)}, f32[16,1,32,128]{3,2,1,0:T(8,128)S(1)}, f32[16,1,32,128...) while((s32[]{:T(128)}, f32[1,128,128]{2,1,0:T(8,128)S(1)}, ...), condition=%wide.region_8.9_spmd.clone, body=%wide.region_6.8_spmd.clone.sunk | while | flops 3223555 | bytes 1574016 | solution.py:121
  27.1 0.4 fusion.503
  28.3 0.4 fusion.503
  29.6 0.4 fusion.503
  30.8 0.4 fusion.503
  32.1 0.4 fusion.503
  33.3 0.4 fusion.503
  34.6 0.4 fusion.503
  35.9 0.4 fusion.503
  38.4 0.4 fusion.503
  40.9 0.4 fusion.503
  42.1 0.4 fusion.503
  44.6 0.4 fusion.503
  46.9 1.9 all-gather.6
  48.9 27.9 %all-gather.7 = bf16[16,129,128]{2,1,0:T(8,128)(2,1)} all-gather(bf16[1,129,128]{2,1,0:T(8,128)(2,1)S(1)} %maximum_bitcast_fusion.3), channel_id=5, replica_groups=mesh['ep_0'=16,'ep_1'=2,'tp'=16] {'ep_0'}, dimensions={0}, use_global_device_ids=true | all-gather | bytes 561408 | tf_op jit(solution)/shard_map/all_gather | solution.py:31
  77.0 20.1 %while.26 = (s32[]{:T(128)}, f32[1,128,128]{2,1,0:T(8,128)S(1)}, f32[16,1,32,128]{3,2,1,0:T(8,128)S(1)}, f32[16,1,32,128]{3,2,1,0:T(8,128)S(1)}, f32[16,1,32,128...) while((s32[]{:T(128)}, f32[1,128,128]{2,1,0:T(8,128)S(1)}, ...), condition=%wide.region_2.3_spmd.clone, body=%wide.region_0.2_spmd.clone.sunk | while | flops 3223555 | bytes 1574016 | solution.py:121
  77.3 0.4 fusion.491
  78.6 0.4 fusion.491
  79.8 0.4 fusion.491
  81.1 0.4 fusion.491
  82.3 0.4 fusion.491
  83.6 0.4 fusion.491
  84.9 0.4 fusion.491
  86.1 0.4 fusion.491
  87.4 0.4 fusion.491
  88.6 0.4 fusion.491
  89.9 0.4 fusion.491
  91.1 0.4 fusion.491
  92.4 0.4 fusion.491
  93.6 0.4 fusion.491
  94.9 0.4 fusion.491
  96.1 0.4 fusion.491
  97.6 8.8 %all-gather.4 = bf16[2,129,128]{2,1,0:T(8,128)(2,1)S(1)} all-gather(bf16[1,129,128]{2,1,0:T(8,128)(2,1)S(1)} %maximum_bitcast_fusion), channel_id=2, replica_groups=mesh['ep_0'=16,'ep_1'=2,'tp'=16] {'ep_1'}, dimensions={0}, use_global_device_ids=true | all-gather | bytes 99072 | tf_op jit(solution)/shard_map/all_gather | solution.py:31
  106.4 0.8 fusion.411
  107.2 1.7 convolution_add_fusion.2
  109.0 1.6 broadcast_in_dim.64
  110.6 6.8 %all-to-all-start.1 = ((bf16[16,32,1,2048]{3,1,2,0:T(8,128)(2,1)}), bf16[16,32,1,2048]{3,1,2,0:T(8,128)(2,1)}, u32[]{:S(2)}, u32[]{:S(2)}) async-start(bf16[16,32,1,2048]{3,1,2,0:T(8,128)(2,1)} %broadcast_in_dim.64), calls=%async_computation.1 | async-start | bytes 4194304 | tf_op jit(solution)/shard_map/all_to_all | solution.py:64
  117.5 0.4 reverse.19
  118.2 26.0 %all-gather.5 = bf16[16,129,128]{2,1,0:T(8,128)(2,1)S(1)} all-gather(bf16[1,129,128]{2,1,0:T(8,128)(2,1)S(1)} %maximum_bitcast_fusion.1), channel_id=3, replica_groups=mesh['ep_0'=16,'ep_1'=2,'tp'=16] {'ep_0'}, dimensions={0}, use_global_device_ids=true | all-gather | bytes 561408 | tf_op jit(solution)/shard_map/all_gather | solution.py:31
  144.3 0.7 multiply_reduce_fusion
  145.0 0.8 fusion.62
  145.8 0.5 copy_bitcast_fusion.1
  146.3 3.4 %all-to-all-done.1 = bf16[16,32,1,2048]{3,1,2,0:T(8,128)(2,1)} async-done(((bf16[16,32,1,2048]{3,1,2,0:T(8,128)(2,1)}), bf16[16,32,1,2048]{3,1,2,0:T(8,128)(2,1)}, u32[]{:S(2)}, u32[]{:S(2)}) %all-to-all-start.1) | async-done | bytes 2097184 | tf_op jit(solution)/shard_map/all_to_all | solution.py:64
  149.7 2.6 %fusion.66 = f32[32,16,224]{2,0,1:T(8,128)S(1)} fusion(bf16[16,32,1,2048]{3,1,2,0:T(8,128)(2,1)} %all-to-all-done.1, bf16[1,2048,224]{1,2,0:T(8,128)(2,1)} %param.31), kind=kOutput, calls=%fused_computation.89 | convolution fusion | flops 469762048 | bytes 3473408 | tf_op jit(solution)/shard_map/scd,df->scf/dot_general | solution.py:161
  152.4 2.4 fusion.71
  154.9 0.7 fusion.63
  155.6 0.5 copy_bitcast_fusion
  156.5 48.7 %all_to_all.20 = bf16[16,128,1024]{1,2,0:T(8,128)(2,1)} all-to-all(bf16[16,128,1024]{1,2,0:T(8,128)(2,1)S(1)} %pad_maximum_fusion), channel_id=1, replica_groups=mesh['ep_0'=16,'ep_1'=2,'tp'=16] {'tp'}, dimensions={0} | all-to-all | bytes 8388608 | tf_op jit(solution)/shard_map/all_to_all | solution.py:88
  205.2 2.9 %reduce.7 = bf16[128,1024]{0,1:T(8,128)(2,1)S(1)} reduce(bf16[16,128,1024]{1,2,0:T(8,128)(2,1)} %all_to_all.20, bf16[]{:T(256)} %constant.138), dimensions={0}, to_apply=%region_19.20.clone | reduce | flops 1966080 | bytes 4456450 | tf_op jit(solution)/shard_map/reduce_sum | solution.py:89
  208.1 0.7 fusion.451
  208.8 15.9 %all-to-all-start.3 = ((bf16[32,16,128]{2,1,0:T(8,128)(2,1)}), bf16[32,16,128]{2,1,0:T(8,128)(2,1)S(1)}, u32[]{:S(2)}, u32[]{:S(2)}) async-start(bf16[32,16,128]{2,1,0:T(8,128)(2,1)} %bitcast.110), calls=%async_computation.3 | async-start | bytes 262144 | tf_op jit(solution)/shard_map/all_to_all | solution.py:288
  225.1 15.4 %all-to-all-done.3 = bf16[32,16,128]{2,1,0:T(8,128)(2,1)S(1)} async-done(((bf16[32,16,128]{2,1,0:T(8,128)(2,1)}), bf16[32,16,128]{2,1,0:T(8,128)(2,1)S(1)}, u32[]{:S(2)}, u32[]{:S(2)}) %all-to-all-start.3) | async-done | bytes 131104 | tf_op jit(solution)/shard_map/all_to_all | solution.py:288
  240.5 0.9 gather_fusion.1
  241.4 0.9 fusion.115
  (417 shorter events, 32.2 us)
Async XLA Ops:
  0.6 154.3 %copy-start = (bf16[1,224,2048]{2,1,0:T(8,128)(2,1)S(1)}, bf16[1,224,2048]{2,1,0:T(8,128)(2,1)}, u32[]{:S(2)}) copy-start(bf16[1,224,2048]{2,1,0:T(8,128)(2,1)} %param.33) | copy-start | bytes 2752516
  1.5 24.1 %copy-start.8 = (f32[2,128]{1,0:T(2,128)S(1)}, f32[2,128]{1,0:T(2,128)}, u32[]{:S(2)}) copy-start(f32[2,128]{1,0:T(2,128)} %param.23) | copy-start | bytes 3076
  1.7 24.0 %copy-start.3 = (bf16[512,128]{1,0:T(8,128)(2,1)S(1)}, bf16[512,128]{1,0:T(8,128)(2,1)}, u32[]{:S(2)}) copy-start(bf16[512,128]{1,0:T(8,128)(2,1)} %param.21) | copy-start | bytes 393220
  1.7 24.0 %copy-start.4 = (bf16[512,128]{1,0:T(8,128)(2,1)S(1)}, bf16[512,128]{1,0:T(8,128)(2,1)}, u32[]{:S(2)}) copy-start(bf16[512,128]{1,0:T(8,128)(2,1)} %param.20) | copy-start | bytes 393220
  1.7 24.0 %copy-start.9 = (f32[1,512]{1,0:T(1,128)S(1)}, f32[1,512]{1,0:T(1,128)}, u32[]{:S(2)}) copy-start(f32[1,512]{1,0:T(1,128)} %param.24) | copy-start | bytes 6148
  6.2 20.2 %copy-start.5 = (bf16[512,128]{1,0:T(8,128)(2,1)S(1)}, bf16[512,128]{1,0:T(8,128)(2,1)}, u32[]{:S(2)}) copy-start(bf16[512,128]{1,0:T(8,128)(2,1)} %param.19) | copy-start | bytes 393220
  6.9 19.6 %copy-start.2 = (bf16[512,128]{1,0:T(8,128)(2,1)S(1)}, bf16[512,128]{1,0:T(8,128)(2,1)}, u32[]{:S(2)}) copy-start(bf16[512,128]{1,0:T(8,128)(2,1)} %param.22) | copy-start | bytes 393220
  8.8 100.0 %all-to-all-start = ((bf16[32,2,1024]{2,1,0:T(2,128)(2,1)}), bf16[32,2,1024]{2,1,0:T(2,128)(2,1)S(1)}, u32[]{:S(2)}, u32[]{:S(2)}) async-start(bf16[32,2,1024]{2,1,0:T(2,128)(2,1)} %reshape.1893), calls=%async_computation | async-start | bytes 262144 | tf_op jit(solution)/shard_map/all_to_all | solution.py:263
  110.6 39.1 %all-to-all-start.1 = ((bf16[16,32,1,2048]{3,1,2,0:T(8,128)(2,1)}), bf16[16,32,1,2048]{3,1,2,0:T(8,128)(2,1)}, u32[]{:S(2)}, u32[]{:S(2)}) async-start(bf16[16,32,1,2048]{3,1,2,0:T(8,128)(2,1)} %broadcast_in_dim.64), calls=%async_computation.1 | async-start | bytes 4194304 | tf_op jit(solution)/shard_map/all_to_all | solution.py:64
  117.4 26.8 %copy-start.6 = (bf16[512,128]{1,0:T(8,128)(2,1)S(1)}, bf16[512,128]{1,0:T(8,128)(2,1)}, u32[]{:S(2)}) copy-start(bf16[512,128]{1,0:T(8,128)(2,1)} %param.19) | copy-start | bytes 393220
  118.1 26.9 %copy-start.1 = (bf16[128,2048]{1,0:T(8,128)(2,1)S(1)}, bf16[128,2048]{1,0:T(8,128)(2,1)}, u32[]{:S(2)}) copy-start(bf16[128,2048]{1,0:T(8,128)(2,1)} %param.26) | copy-start | bytes 1572868
  118.1 26.9 %copy-start.11 = (f32[128]{0:T(128)S(1)}, f32[128]{0:T(128)}, u32[]{:S(2)}) copy-start(f32[128]{0:T(128)} %param.25) | copy-start | bytes 1540
  149.7 2.6 %copy-start.12 = (bf16[1,2048,224]{1,2,0:T(8,128)(2,1)S(1)}, bf16[1,2048,224]{1,2,0:T(8,128)(2,1)}, u32[]{:S(2)}) copy-start(bf16[1,2048,224]{1,2,0:T(8,128)(2,1)} %param.32) | copy-start | bytes 2752516
  205.2 19.5 %copy-start.7 = (s32[128,2]{0,1:T(2,128)S(1)}, s32[128,2]{0,1:T(2,128)}, u32[]{:S(2)}) copy-start(s32[128,2]{0,1:T(2,128)} %param.29) | copy-start | bytes 3076
  205.2 19.8 %copy-start.10 = (f32[128,2]{0,1:T(2,128)S(1)}, f32[128,2]{0,1:T(2,128)}, u32[]{:S(2)}) copy-start(f32[128,2]{0,1:T(2,128)} %param.30) | copy-start | bytes 3076
  208.8 31.7 %all-to-all-start.3 = ((bf16[32,16,128]{2,1,0:T(8,128)(2,1)}), bf16[32,16,128]{2,1,0:T(8,128)(2,1)S(1)}, u32[]{:S(2)}, u32[]{:S(2)}) async-start(bf16[32,16,128]{2,1,0:T(8,128)(2,1)} %bitcast.110), calls=%async_computation.3 | async-start | bytes 262144 | tf_op jit(solution)/shard_map/all_to_all | solution.py:288
where the time goes:
time: 243 us; the launch traced here: 242 us
  blocking collectives  113 us (47%)
  starting transfers between devices  39.4 us (16%)
  other arithmetic  31.5 us (13%)
  matrix products  25.2 us (10%)
  waiting for transfers between devices  18.8 us (8%)
  local copies, waits for them, and re-layouts  10.9 us (4%)
    all_gather x4, blocking collectives, collected_together(): both, at, found = (lax.all_gather(jnp.concatenate(lines), axis), 0, {})  64.5 us
    all_to_all x1, blocking collectives, summed_on_arrival(): lax.all_to_all(blocks, axis, split_axis=0, concat_axis=0, tiled=True)  48.7 us
    all_to_all x1, starting transfers between devices, per_device(): lax.all_to_all(outgoing, EP, split_axis=0, concat_axis=0, tiled=True)  16.7 us
    all_to_all x1, starting transfers between devices, per_device(): lax.all_to_all(outgoing_back, EP, split_axis=0, concat_axis=0, tiled=True)  15.9 us
    all_to_all x1, waiting for transfers between devices, per_device(): lax.all_to_all(outgoing_back, EP, split_axis=0, concat_axis=0, tiled=True)  15.4 us
    dot_general x32, other arithmetic, advance(): scores = jnp.einsum('htk,hsk,htsk->hts', query_block, key_block, decays)  12.1 us
    all_to_all x1, starting transfers between devices, from_everyone(): lax.all_to_all(jnp.broadcast_to(shard[None], (peers, *shard.shape)), axis...  6.81 us
    exp x32, other arithmetic, advance(): decays = jnp.exp(jnp.where(lower_tri, relative, NEG_BIG))  6.69 us
  transfers between devices with their start and end apart: 3, of which 2 were waited for; matrix products, arithmetic and copies ran while one was open for 19% of the time, Pallas kernels for 0%

commit v1 on v0

v1 whole, which is shorter than its diff:
```python
import functools

import jax
import jax.numpy as jnp
from jax import lax
from jax.experimental import pallas as pl
from jax.experimental.pallas import tpu as pltpu
from jax.sharding import Mesh
from jax.sharding import PartitionSpec as P

EPS = 1e-06
CAP = 16
LANES = 128
CHUNK = 128
MESH = pl.DeviceIdType.MESH
F32 = jnp.float32
BF16 = jnp.bfloat16


def nn(a, b):
    return lax.dot_general(a, b, (((1,), (0,)), ((), ())), preferred_element_type=F32)


def nt(a, b):
    return lax.dot_general(a, b, (((1,), (1,)), ((), ())), preferred_element_type=F32)


def tn(a, b):
    return lax.dot_general(a, b, (((0,), (0,)), ((), ())), preferred_element_type=F32)


def iota(shape, dim):
    return lax.broadcasted_iota(jnp.int32, shape, dim)


def three_parts(a):
    hi = a.astype(BF16).astype(F32)
    rest = a - hi
    mid = rest.astype(BF16).astype(F32)
    return hi, mid, (rest - mid).astype(BF16).astype(F32)


def send(src, dst, send_sem, recv_sem, device):
    copy = pltpu.make_async_remote_copy(
        src_ref=src,
        dst_ref=dst,
        send_sem=send_sem,
        recv_sem=recv_sem,
        device_id=device,
        device_id_type=MESH,
    )
    copy.start()
    return copy


class Ring:
    def __init__(self, z, c, y, x):
        self.z, self.c, self.y, self.x = z, c, y, x

    def along(self, axis, step):
        return lax.rem((self.x if axis == 0 else self.y) + step, 4)

    def device(self, axis, step):
        there = self.along(axis, step)
        return (self.z, self.c, self.y, there) if axis == 0 else (self.z, self.c, there, self.x)


class Gather:
    ORDER = (0, 3, 1, 2)

    def __init__(self, ring, buf, send_sems, recv_sems):
        self.ring, self.buf = ring, buf
        self.send_sems, self.recv_sems = send_sems, recv_sems
        self.rows = buf.shape[2]
        self.sent = []

    def block(self, half, first, second, part):
        a, b = self.ring.along(half, first), self.ring.along(1 - half, second)
        y, x = (b, a) if half == 0 else (a, b)
        n = self.rows // 2
        start, size = {None: (0, n), 0: (0, n // 2), 1: (n // 2, n // 2)}[part]
        return self.buf.at[y, x, pl.ds(half * n + start, size), :]

    def go(self, half, axis, step, block, k):
        self.sent.append(
            send(
                block,
                block,
                self.send_sems.at[half, k],
                self.recv_sems.at[half, k],
                self.ring.device(axis, step),
            )
        )

    def arrived(self, half, block, k):
        pltpu.make_async_copy(block, block, self.recv_sems.at[half, k]).wait()

    def second(self, half, n):
        first = self.ORDER[n]
        block = self.block(half, first, 0, None)
        self.go(half, 1 - half, 1, block, 4 + 4 * n)
        self.go(half, 1 - half, 3, block, 5 + 4 * n)

    def start(self):
        for half in range(2):
            block = self.block(half, 0, 0, None)
            self.go(half, half, 1, block, 0)
            self.go(half, half, 3, block, 1)
        for half in range(2):
            self.second(half, 0)

    def near(self):
        for half in range(2):
            self.arrived(half, self.block(half, 3, 0, None), 0)
            self.go(half, half, 1, self.block(half, 3, 0, 0), 2)
            self.arrived(half, self.block(half, 1, 0, None), 1)
            self.go(half, half, 3, self.block(half, 1, 0, 1), 3)
        for half in range(2):
            self.second(half, 1)
            self.second(half, 2)

    def far(self):
        for half in range(2):
            self.arrived(half, self.block(half, 2, 0, 0), 2)
            self.arrived(half, self.block(half, 2, 0, 1), 3)
            self.second(half, 3)

    def relay(self, n):
        first = self.ORDER[n]
        for half in range(2):
            self.arrived(half, self.block(half, first, 3, None), 4 + 4 * n)
            self.go(half, 1 - half, 1, self.block(half, first, 3, 0), 6 + 4 * n)
            self.arrived(half, self.block(half, first, 1, None), 5 + 4 * n)
            self.go(half, 1 - half, 3, self.block(half, first, 1, 1), 7 + 4 * n)

    def finish(self, half):
        for n in range(4):
            first = self.ORDER[n]
            self.arrived(half, self.block(half, first, 2, 0), 6 + 4 * n)
            self.arrived(half, self.block(half, first, 2, 1), 7 + 4 * n)

    def drain(self):
        for copy in self.sent:
            copy.wait_send()


class Scatter:
    ORDER = (2, 1, 3, 0)

    def __init__(self, ring, part, far, near, last_far, last_near, out, send_sems, recv_sems):
        self.ring, self.part, self.out = ring, part, out
        self.far, self.near, self.last_far, self.last_near = far, near, last_far, last_near
        self.send_sems, self.recv_sems = send_sems, recv_sems
        self.n = part.shape[2] // 2
        self.sent = []

    def block(self, half, first, second, lo, size):
        axis = 1 - half
        a, b = self.ring.along(axis, first), self.ring.along(1 - axis, second)
        y, x = (a, b) if axis == 1 else (b, a)
        return self.part.at[y, x, pl.ds(half * self.n + lo, size), :]

    def go(self, half, axis, step, src, dst, k):
        self.sent.append(
            send(
                src,
                dst,
                self.send_sems.at[half, k],
                self.recv_sems.at[half, k],
                self.ring.device(axis, step),
            )
        )

    def arrived(self, half, ref, k):
        pltpu.make_async_copy(ref, ref, self.recv_sems.at[half, k]).wait()

    def start(self, half):
        q = self.n // 2
        for m in range(4):
            o = self.ORDER[m]
            self.go(half, 1 - half, 1, self.block(half, 2, o, 0, q), self.far.at[half, 0, m], 4 * m)
            self.go(half, 1 - half, 3, self.block(half, 2, o, q, q), self.far.at[half, 1, m], 4 * m + 1)

    def pass_on(self, half, m):
        q, o = self.n // 2, self.ORDER[m]
        for way, step in ((0, 1), (1, 3)):
            come = self.far.at[half, way, m]
            self.arrived(half, come, 4 * m + way)
            mine = self.block(half, step, o, way * q, q)
            mine[...] = (mine[...].astype(F32) + come[...].astype(F32)).astype(BF16)
            self.go(
                half,
                1 - half,
                step,
                self.block(half, step, o, 0, self.n),
                self.near.at[half, way, m],
                4 * m + 2 + way,
            )

    def collect(self, half, m):
        o = self.ORDER[m]
        for way in range(2):
            self.arrived(half, self.near.at[half, way, m], 4 * m + 2 + way)
        mine = self.block(half, 0, o, 0, self.n)
        total = mine[...].astype(F32) + self.near[half, 0, m].astype(F32)
        mine[...] = (total + self.near[half, 1, m].astype(F32)).astype(BF16)
        q = self.n // 2
        if m == 0:
            self.go(half, half, 1, self.block(half, 0, 2, 0, q), self.last_far.at[half, 0], 16)
            self.go(half, half, 3, self.block(half, 0, 2, q, q), self.last_far.at[half, 1], 17)

    def last_pass(self, half):
        q = self.n // 2
        for way, step in ((0, 1), (1, 3)):
            come = self.last_far.at[half, way]
            self.arrived(half, come, 16 + way)
            mine = self.block(half, 0, step, way * q, q)
            mine[...] = (mine[...].astype(F32) + come[...].astype(F32)).astype(BF16)
            self.go(
                half,
                half,
                step,
                self.block(half, 0, step, 0, self.n),
                self.last_near.at[half, way],
                18 + way,
            )

    def end(self, half):
        for way in range(2):
            self.arrived(half, self.last_near.at[half, way], 18 + way)
        total = self.block(half, 0, 0, 0, self.n)[...].astype(F32)
        total = total + self.last_near[half, 0].astype(F32) + self.last_near[half, 1].astype(F32)
        self.out[pl.ds(half * self.n, self.n), :] = total.astype(BF16)

    def drain(self):
        for copy in self.sent:
            copy.wait_send()


def kernel(
    ep_count,
    q_ref,
    right_ref,
    left_ref,
    v_ref,
    bounds_ref,
    spikes_ref,
    gain_ref,
    emit_ref,
    rows_ref,
    rows_gain_ref,
    ids_ref,
    shares_ref,
    switch_ref,
    widen_ref,
    shrink_ref,
    out_a_ref,
    out_b_ref,
    switch_buf,
    widen_buf,
    shrink_buf,
    emit_buf,
    outgoing,
    ebuf,
    part,
    far,
    near,
    last_far,
    last_near,
    expert_out,
    returned,
    picks,
    intra,
    query_f,
    query_b,
    added_f,
    added_b,
    chunk_decay,
    leg1_out,
    leg1_in,
    leg2_out,
    leg2_in,
    mbuf,
    load_sems,
    all_send,
    all_recv,
    eg_send,
    eg_recv,
    mg_send,
    mg_recv,
    rs_send,
    rs_recv,
):
    z, c = lax.axis_index("z"), lax.axis_index("c")
    y, x = lax.axis_index("y"), lax.axis_index("x")
    s, t = 2 * z + c, 4 * y + x
    ring = Ring(z, c, y, x)
    tok = q_ref.shape[0]
    chunks = tok // CHUNK
    rows_b = rows_ref.shape[0]
    slots = ep_count * CAP

    def ep_peer(k):
        other = lax.rem(s + k, ep_count)
        return other, (lax.div(other, 2), lax.rem(other, 2), y, x)

    def tp_peer(k):
        other = lax.rem(t + k, 16)
        return other, (z, c, lax.div(other, 4), lax.rem(other, 4))

    barrier = pltpu.get_barrier_semaphore()

    def greet_ep(k, _):
        pl.semaphore_signal(barrier, inc=1, device_id=ep_peer(k)[1], device_id_type=MESH)
        return _

    def greet_tp(k, _):
        pl.semaphore_signal(barrier, inc=1, device_id=tp_peer(k)[1], device_id_type=MESH)
        return _

    lax.fori_loop(1, ep_count, greet_ep, 0)
    lax.fori_loop(1, 16, greet_tp, 0)

    loads = [
        pltpu.make_async_copy(src, dst, load_sems.at[i])
        for i, (src, dst) in enumerate(
            (
                (switch_ref.at[0], switch_buf),
                (widen_ref.at[0], widen_buf),
                (shrink_ref.at[0], shrink_buf),
                (
                    emit_ref.at[:, pl.ds(pl.multiple_of(t * LANES, LANES), LANES)],
                    emit_buf.at[pl.ds(pl.multiple_of(t * LANES, LANES), LANES), :],
                ),
            )
        )
    ]
    for load in loads:
        load.start()

    width = rows_ref.shape[1]
    square = jnp.zeros((rows_b, LANES), F32)
    for k in range(width // LANES):
        piece = rows_ref[:, k * LANES : (k + 1) * LANES].astype(F32)
        square = square + piece * piece
    mean = jnp.sum(square, axis=1, keepdims=True) / width
    own_columns = pl.ds(pl.multiple_of(t * LANES, LANES), LANES)
    normed = rows_ref[:, own_columns].astype(F32) * lax.rsqrt(mean + EPS)
    normed = (normed * rows_gain_ref[:, own_columns]).astype(BF16)
    experts = iota((ep_count, rows_b), 0)
    pick0 = ids_ref[0:1, :] == experts
    pick1 = ids_ref[1:2, :] == experts
    named = (pick0 | pick1).astype(F32).astype(BF16)
    earlier = (iota((rows_b, rows_b), 0) < iota((rows_b, rows_b), 1)).astype(F32).astype(BF16)
    rank = nn(named, earlier)
    at_slot = rank.astype(jnp.int32)[:, None, :] == iota((ep_count, CAP, rows_b), 1)
    ones = jnp.where(at_slot, 1.0, 0.0)
    for k, pick in enumerate((pick0, pick1)):
        chosen = ones * jnp.where(pick, 1.0, 0.0)[:, None, :]
        picks[k] = chosen.reshape(slots, rows_b).astype(BF16)
    outgoing[...] = nn(picks[0] + picks[1], normed).astype(BF16)
    own_slots = pl.ds(pl.multiple_of(s * CAP, CAP), CAP)
    ebuf[y, x, own_slots, :] = outgoing[own_slots, :]

    pl.semaphore_wait(barrier, ep_count - 1 + 15)

    def dispatch(k, _):
        other, device = ep_peer(k)
        send(
            outgoing.at[pl.ds(pl.multiple_of(other * CAP, CAP), CAP), :],
            ebuf.at[y, x, own_slots, :],
            all_send.at[0],
            all_recv.at[0],
            device,
        )
        return _

    lax.fori_loop(1, ep_count, dispatch, 0)

    tri = iota((CHUNK, CHUNK), 0) >= iota((CHUNK, CHUNK), 1)
    tri_t = iota((CHUNK, CHUNK), 0) <= iota((CHUNK, CHUNK), 1)
    for n in range(chunks):
        at = slice(n * CHUNK, (n + 1) * CHUNK)
        query = q_ref[at, :].astype(F32)
        query = query * jax.nn.sigmoid(query)
        values = v_ref[at, :]
        spike = spikes_ref[0:1, at]
        scores = []
        for d, (pre_ref, mask, queries, added) in enumerate(
            ((right_ref, tri, query_f, added_f), (left_ref, tri_t, query_b, added_b))
        ):
            pre = pre_ref[at, :].astype(F32)
            bound = bounds_ref[d : d + 1, :]
            gap = 1.0 - bound
            log_decay = jnp.log(bound + gap * jax.nn.sigmoid(pre))
            key = gap * jax.nn.sigmoid(-pre)
            split = jnp.concatenate(three_parts(log_decay), axis=1).astype(BF16)
            summed = nn(jnp.where(mask, 1.0, 0.0).astype(BF16), split)
            total = summed[:, :LANES] + summed[:, LANES : 2 * LANES] + summed[:, 2 * LANES :]
            total = total + jnp.sum(jnp.where(mask, spike, 0.0), axis=1, keepdims=True)
            whole = total[CHUNK - 1 : CHUNK, :] if d == 0 else total[0:1, :]
            middle = total[CHUNK // 2 : CHUNK // 2 + 1, :]
            near_q = (query * jnp.exp(total - middle)).astype(BF16)
            near_k = (key * jnp.exp(middle - total)).astype(BF16)
            scores.append(jnp.where(mask, nt(near_q, near_k), 0.0))
            queries[at, :] = (query * jnp.exp(total)).astype(BF16)
            added[n] = tn(values, (key * jnp.exp(whole - total)).astype(BF16))
            chunk_decay[d, n] = whole
        intra[at, :] = nn((scores[0] + scores[1]).astype(BF16), values)

    z_count = ep_count // 2
    rows_s = LANES // z_count
    for d, (added, order) in enumerate(
        ((added_f, range(chunks)), (added_b, range(chunks - 1, -1, -1)))
    ):
        state, decay = None, None
        for n in order:
            state = added[n] if state is None else state * jnp.exp(chunk_decay[d, n]) + added[n]
            decay = chunk_decay[d, n] if decay is None else decay + chunk_decay[d, n]
        hi, mid, lo = three_parts(decay)
        row = iota((8, LANES), 0)
        tail = jnp.where(row == 0, hi, jnp.where(row == 1, mid, jnp.where(row == 2, lo, 0.0)))
        tail = jnp.broadcast_to(tail[None], (z_count, 8, LANES))
        leg1_out[:, d] = jnp.concatenate(
            [state.reshape(z_count, rows_s, LANES), tail], axis=1
        ).astype(BF16)

    def leg1(k, _):
        other, device = ep_peer(k)
        send(
            leg1_out.at[lax.div(other, 2), lax.rem(other, 2)],
            leg1_in.at[s],
            all_send.at[1],
            all_recv.at[1],
            device,
        )
        return _

    lax.fori_loop(1, ep_count, leg1, 0)
    leg1_in[s] = leg1_out[z, c]

    own_rows = pl.ds(pl.multiple_of(t * LANES, LANES), LANES)

    def deal(k, _):
        other, device = tp_peer(k)
        send(
            emit_ref.at[:, pl.ds(pl.multiple_of(other * LANES, LANES), LANES)],
            emit_buf.at[own_rows, :],
            all_send.at[4],
            all_recv.at[4],
            device,
        )
        return _

    def all_arrived(ref, k):
        pltpu.make_async_copy(ref, ref, all_recv.at[k]).wait()

    slots_in = ebuf.at[y, x, pl.ds(0, slots - CAP), :]
    all_arrived(slots_in, 0)
    gather_e = Gather(ring, ebuf, eg_send, eg_recv)
    gather_e.start()
    gather_e.near()

    all_arrived(leg1_in.at[pl.ds(0, ep_count - 1)], 1)
    carried = jnp.zeros((rows_s, LANES), F32)
    for n in range(ep_count):
        i = jnp.where(c == 0, n, ep_count - 1 - n)
        tile = leg1_in[i].astype(F32)
        leg2_out[i] = carried.astype(BF16)
        decay = tile[rows_s : rows_s + 1] + tile[rows_s + 1 : rows_s + 2] + tile[rows_s + 2 : rows_s + 3]
        carried = carried * jnp.exp(decay) + tile[:rows_s]

    def leg2(k, _):
        other, device = ep_peer(k)
        send(leg2_out.at[other], leg2_in.at[s], all_send.at[2], all_recv.at[2], device)
        return _

    lax.fori_loop(1, ep_count, leg2, 0)
    leg2_in[s] = leg2_out[s]

    gather_e.far()
    lax.fori_loop(1, 16, deal, 0)
    for n in range(3):
        gather_e.relay(n)

    all_arrived(leg2_in.at[pl.ds(0, ep_count - 1)], 2)
    entries = [
        jnp.concatenate([leg2_in[2 * k + d].astype(F32) for k in range(z_count)], axis=0)
        for d in range(2)
    ]
    for d, (added, queries, order) in enumerate(
        ((added_f, query_f, range(chunks)), (added_b, query_b, range(chunks - 1, -1, -1)))
    ):
        state = entries[d]
        for n in order:
            at = slice(n * CHUNK, (n + 1) * CHUNK)
            intra[at, :] += nt(queries[at, :], state.astype(BF16))
            state = state * jnp.exp(chunk_decay[d, n]) + added[n]
    mixed = intra[...]
    mixed = mixed * lax.rsqrt(jnp.mean(mixed * mixed, axis=1, keepdims=True) + EPS)
    mbuf[y, x] = (mixed * gain_ref[...]).astype(BF16)
    gather_e.relay(3)
    gather_m = Gather(ring, mbuf, mg_send, mg_recv)

    for load in loads[:3]:
        load.wait()
    scatter = Scatter(
        ring, part, far, near, last_far, last_near, expert_out, rs_send, rs_recv
    )
    half_rows = slots // 2
    for half in range(2):
        gather_e.finish(half)
        at = pl.ds(half * half_rows, half_rows)
        tokens = jnp.concatenate([ebuf[k // 4, k % 4, at, :] for k in range(16)], axis=1)
        opened = nt(tokens, switch_buf[...])
        opened = opened * jax.nn.sigmoid(opened)
        hidden = (opened * nt(tokens, widen_buf[...])).astype(BF16)
        for k in range(4):
            product = nn(hidden, shrink_buf[:, k * 512 : (k + 1) * 512]).astype(BF16)
            for m in range(4):
                part[k, m, at, :] = product[:, m * LANES : (m + 1) * LANES]
        scatter.start(half)

    gather_m.start()
    for m in range(4):
        scatter.pass_on(0, m)
        scatter.pass_on(1, m)
    gather_m.near()
    for m in range(4):
        scatter.collect(0, m)
        scatter.collect(1, m)
    gather_m.far()
    for half in range(2):
        scatter.last_pass(half)
    for half in range(2):
        scatter.end(half)

    def give_back(k, _):
        other, device = ep_peer(k)
        send(
            expert_out.at[pl.ds(pl.multiple_of(other * CAP, CAP), CAP), :],
            returned.at[own_slots, :],
            all_send.at[3],
            all_recv.at[3],
            device,
        )
        return _

    lax.fori_loop(1, ep_count, give_back, 0)
    returned[own_slots, :] = expert_out[own_slots, :]

    for n in range(4):
        gather_m.relay(n)
    loads[3].wait()
    all_arrived(emit_buf.at[pl.ds(0, 15 * LANES), :], 4)
    for half in range(2):
        gather_m.finish(half)
        at = pl.ds(half * (tok // 2), tok // 2)
        heads = jnp.concatenate([mbuf[k // 4, k % 4, at, :] for k in range(16)], axis=1)
        out_a_ref[at, :] = nn(heads, emit_buf[...]).astype(BF16)

    all_arrived(returned.at[pl.ds(0, slots - CAP), :], 3)
    results = returned[...]
    same = iota((rows_b, rows_b), 0) == iota((rows_b, rows_b), 1)
    mixed_b = jnp.zeros((rows_b, LANES), F32)
    for k in range(2):
        share = jnp.sum(jnp.where(same, shares_ref[k : k + 1, :], 0.0), axis=1, keepdims=True)
        mixed_b = mixed_b + tn(picks[k], results) * share
    out_b_ref[...] = mixed_b.astype(BF16)

    def all_sent(ref, k):
        pltpu.make_async_copy(ref, ref, all_send.at[k]).wait()

    all_sent(outgoing.at[pl.ds(0, slots - CAP), :], 0)
    all_sent(leg1_in.at[pl.ds(0, ep_count - 1)], 1)
    all_sent(leg2_in.at[pl.ds(0, ep_count - 1)], 2)
    all_sent(returned.at[pl.ds(0, slots - CAP), :], 3)
    all_sent(emit_buf.at[pl.ds(0, 15 * LANES), :], 4)
    gather_e.drain()
    gather_m.drain()
    scatter.drain()


def per_device(*args):
    (q, right, left, v, bounds, spikes, gain, emit, rows, rows_gain, ids, shares, switch, widen, shrink) = args
    ep_count = lax.axis_size("z") * 2
    tok, rows_b, width = q.shape[0], rows.shape[0], rows.shape[1]
    hidden = switch.shape[2]
    slots = ep_count * CAP
    chunks = tok // CHUNK
    z_count = ep_count // 2
    rows_s = LANES // z_count
    n, r = slots // 2, slots // 4
    vmem = pl.BlockSpec(memory_space=pltpu.VMEM)
    anywhere = pl.BlockSpec(memory_space=pl.ANY)
    dma = pltpu.SemaphoreType.DMA
    return pl.pallas_call(
        functools.partial(kernel, ep_count),
        out_shape=(
            jax.ShapeDtypeStruct((tok, LANES), BF16),
            jax.ShapeDtypeStruct((rows_b, LANES), BF16),
        ),
        in_specs=[vmem] * 7 + [anywhere] + [vmem] * 4 + [anywhere] * 3,
        out_specs=(vmem, vmem),
        scratch_shapes=[
            pltpu.VMEM((hidden, width), BF16),
            pltpu.VMEM((hidden, width), BF16),
            pltpu.VMEM((hidden, width), BF16),
            pltpu.VMEM((width, LANES), BF16),
            pltpu.VMEM((slots, LANES), BF16),
            pltpu.VMEM((4, 4, slots, LANES), BF16),
            pltpu.VMEM((4, 4, slots, LANES), BF16),
            pltpu.VMEM((2, 2, 4, r, LANES), BF16),
            pltpu.VMEM((2, 2, 4, n, LANES), BF16),
            pltpu.VMEM((2, 2, r, LANES), BF16),
            pltpu.VMEM((2, 2, n, LANES), BF16),
            pltpu.VMEM((slots, LANES), BF16),
            pltpu.VMEM((slots, LANES), BF16),
            pltpu.VMEM((2, slots, rows_b), BF16),
            pltpu.VMEM((tok, LANES), F32),
            pltpu.VMEM((tok, LANES), BF16),
            pltpu.VMEM((tok, LANES), BF16),
            pltpu.VMEM((chunks, LANES, LANES), F32),
            pltpu.VMEM((chunks, LANES, LANES), F32),
            pltpu.VMEM((2, chunks, 1, LANES), F32),
            pltpu.VMEM((z_count, 2, rows_s + 8, LANES), BF16),
            pltpu.VMEM((ep_count, rows_s + 8, LANES), BF16),
            pltpu.VMEM((ep_count, rows_s, LANES), BF16),
            pltpu.VMEM((ep_count, rows_s, LANES), BF16),
            pltpu.VMEM((4, 4, tok, LANES), BF16),
            dma((4,)),
            dma((5,)),
            dma((5,)),
            dma((2, 20)),
            dma((2, 20)),
            dma((2, 20)),
            dma((2, 20)),
            dma((2, 20)),
            dma((2, 20)),
        ],
        compiler_params=pltpu.CompilerParams(collective_id=0, has_side_effects=True),
    )(
        q,
        right,
        left,
        v,
        bounds,
        spikes,
        gain.reshape(1, -1),
        emit,
        rows,
        rows_gain.reshape(1, -1),
        ids.T,
        shares.T,
        switch.transpose(0, 2, 1),
        widen.transpose(0, 2, 1),
        shrink,
    )


def solution(mesh):
    ep, tp = mesh.shape["ep"], mesh.shape["tp"]
    split = Mesh(mesh.devices.reshape(ep // 2, 2, tp // 4, 4), ("z", "c", "y", "x"))
    e, f = ("z", "c"), ("y", "x")
    return jax.shard_map(
        per_device,
        mesh=split,
        in_specs=(
            P(e, f),
            P(e, f),
            P(e, f),
            P(e, f),
            P(None, f),
            P(f, e),
            P(f),
            P(f, None),
            P(e, None),
            P(),
            P(e, None),
            P(e, None),
            P(e, None, f),
            P(e, None, f),
            P(e, f, None),
        ),
        out_specs=(P(e, f), P(e, f)),
        check_vma=False,
    )
```

time: 243 us -> 89.5 us (0.37)
  blocking collectives: 113 us -> 0 us
  Pallas kernels: 0 us -> 86.5 us
  starting transfers between devices: 39.4 us -> 0 us
  other arithmetic: 31.5 us -> 0 us
  matrix products: 25.2 us -> 0 us
  waiting for transfers between devices: 18.8 us -> 0 us
  local copies, waits for them, and re-layouts: 10.9 us -> 2.19 us
    pallas_call x0 -> x1, Pallas kernels: none -> 86.5 us  [per_device(): pl.pallas_call(functools.partial(kernel, ep_count), out_shape=(jax.ShapeD...]
    all_gather x4 -> x0, blocking collectives: 64.5 us -> none  [collected_together(): both, at, found = (lax.all_gather(jnp.concatenate(lines), axis), 0, {})]
    all_to_all x1 -> x0, blocking collectives: 48.7 us -> none  [summed_on_arrival(): lax.all_to_all(blocks, axis, split_axis=0, concat_axis=0, tiled=True)]
    all_to_all x3 -> x0, starting transfers between devices: 39.4 us -> none  [the longest x1 16.7 us: per_device(): lax.all_to_all(outgoing, EP, split_axis=0, concat_axis=0, tiled=True)]
    dot_general x102 -> x0, matrix products: 25.2 us -> none  [the longest x32 6.59 us: advance(): jnp.einsum('qfw,qfa->qwa', key_block * jnp.exp(block_final_state - cumula...]
    all_to_all x3 -> x0, waiting for transfers between devices: 18.8 us -> none  [the longest x1 15.4 us: per_device(): lax.all_to_all(outgoing_back, EP, split_axis=0, concat_axis=0, tiled=True)]
    dot_general x32 -> x0, other arithmetic: 12.1 us -> none  [advance(): scores = jnp.einsum('htk,hsk,htsk->hts', query_block, key_block, decays)]
    exp x38 -> x0, other arithmetic: 7.58 us -> none  [the longest x32 6.69 us: advance(): decays = jnp.exp(jnp.where(lower_tri, relative, NEG_BIG))]
  transfers between devices with their start and end apart: 3 -> 0, of which waited for: 2 -> 0; matrix products, arithmetic and copies ran while one was open for 19% -> 0% of each run, Pallas kernels for 0% -> 0%
where the time goes in v1:
time: 89.5 us; the launch traced here: 89.4 us
  Pallas kernels  86.5 us (97%)
  local copies, waits for them, and re-layouts  2.19 us (2%)
    pallas_call x1, Pallas kernels, per_device(): pl.pallas_call(functools.partial(kernel, ep_count), out_shape=(jax.ShapeD...  86.5 us
    unnamed x4, local copies, waits for them, and re-layouts  2.19 us

profile of v1, /device:TPU:1, one launch (start us, length us, event | category | flops | bytes accessed | tf_op | source)
XLA Modules:
  0.0 89.4 jit_solution(16167910010541791193)
XLA Ops:
  0.6 86.5 %shard_map.158 = (bf16[512,128]{1,0:T(8,128)(2,1)}, bf16[128,128]{1,0:T(8,128)(2,1)}) custom-call(bf16[512,128]{1,0:T(8,128)(2,1)} %q_ref.1, bf16[512,128]{1,0:T(8,128)(2,1)} %right_ref.1, bf16[512,128]{1,0:T(8,128)(2,1)} %left_ref.1, bf16[512,128]{1,0:T(8,128)(2,1)} %v_ref.1, f32[2,128]{1,0:T(2,128)} %bounds_ref.1, f32[1,512]{1,0:T(1,128)} %spikes_ref.1, ...), custom_call_target="tpu_custom_call" | custom-call | tf_op jit(solution)/shard_map/pallas_call | solution.py:597
  87.2 0.0 copy-start
  87.2 1.6 %copy.19 = bf16[512,128]{1,0:T(8,128)(2,1)} copy(bf16[512,128]{1,0:T(8,128)(2,1)} %get-tuple-element.4) | data formatting | bytes 262144
  88.7 0.0 copy-done
  88.7 0.6 copy.20
Async XLA Ops:
  87.2 1.6 %copy-start = (bf16[128,128]{1,0:T(8,128)(2,1)S(1)}, bf16[128,128]{1,0:T(8,128)(2,1)}, u32[]{:S(2)}) copy-start(bf16[128,128]{1,0:T(8,128)(2,1)} %get-tuple-element.5) | copy-start | bytes 98308

commit v2 on v1

v2 whole, which is shorter than its diff:
```python
import functools

import jax
import jax.numpy as jnp
from jax import lax
from jax.experimental import pallas as pl
from jax.experimental.pallas import tpu as pltpu
from jax.sharding import Mesh
from jax.sharding import PartitionSpec as P

EPS = 1e-06
CAP = 16
LANES = 128
CHUNK = 128
DIRECT_GATHER = (False, True)
DIRECT_SCATTER = (False, False)
MESH = pl.DeviceIdType.MESH
F32 = jnp.float32
BF16 = jnp.bfloat16


def nn(a, b):
    return lax.dot_general(a, b, (((1,), (0,)), ((), ())), preferred_element_type=F32)


def nt(a, b):
    return lax.dot_general(a, b, (((1,), (1,)), ((), ())), preferred_element_type=F32)


def tn(a, b):
    return lax.dot_general(a, b, (((0,), (0,)), ((), ())), preferred_element_type=F32)


def iota(shape, dim):
    return lax.broadcasted_iota(jnp.int32, shape, dim)


def three_parts(a):
    hi = a.astype(BF16).astype(F32)
    rest = a - hi
    mid = rest.astype(BF16).astype(F32)
    return hi, mid, (rest - mid).astype(BF16).astype(F32)


def send(src, dst, send_sem, recv_sem, device):
    copy = pltpu.make_async_remote_copy(
        src_ref=src,
        dst_ref=dst,
        send_sem=send_sem,
        recv_sem=recv_sem,
        device_id=device,
        device_id_type=MESH,
    )
    copy.start()
    return copy


class Ring:
    def __init__(self, z, c, y, x):
        self.z, self.c, self.y, self.x = z, c, y, x

    def along(self, axis, step):
        return lax.rem((self.x if axis == 0 else self.y) + step, 4)

    def device(self, axis, step):
        there = self.along(axis, step)
        return (self.z, self.c, self.y, there) if axis == 0 else (self.z, self.c, there, self.x)


class Gather:
    ORDER = (0, 3, 1, 2)

    def __init__(self, ring, buf, base, rows, direct, send_sems, recv_sems):
        self.ring, self.buf, self.base, self.rows, self.direct = ring, buf, base, rows, direct
        self.send_sems, self.recv_sems = send_sems, recv_sems
        self.sent = []

    def block(self, half, first, second, part):
        a, b = self.ring.along(half, first), self.ring.along(1 - half, second)
        y, x = (b, a) if half == 0 else (a, b)
        n = self.rows // 2
        start, size = {None: (0, n), 0: (0, n // 2), 1: (n // 2, n // 2)}[part]
        return self.buf.at[y, x, pl.ds(self.base + half * n + start, size), :]

    def go(self, half, axis, step, block, k):
        self.sent.append(
            send(
                block,
                block,
                self.send_sems.at[half, k],
                self.recv_sems.at[half, k],
                self.ring.device(axis, step),
            )
        )

    def arrived(self, half, block, k):
        pltpu.make_async_copy(block, block, self.recv_sems.at[half, k]).wait()

    def second(self, half, n):
        first = self.ORDER[n]
        block = self.block(half, first, 0, None)
        self.go(half, 1 - half, 1, block, 4 + 4 * n)
        self.go(half, 1 - half, 3, block, 5 + 4 * n)
        if self.direct:
            self.go(half, 1 - half, 2, block, 6 + 4 * n)

    def start(self):
        for half in range(2):
            block = self.block(half, 0, 0, None)
            self.go(half, half, 1, block, 0)
            self.go(half, half, 3, block, 1)
            self.go(half, half, 2, block, 2)
        for half in range(2):
            self.second(half, 0)

    def near(self):
        for half in range(2):
            self.arrived(half, self.block(half, 3, 0, None), 0)
            self.second(half, 1)
            self.arrived(half, self.block(half, 1, 0, None), 1)
            self.second(half, 2)

    def far(self):
        for half in range(2):
            self.arrived(half, self.block(half, 2, 0, None), 2)
            self.second(half, 3)

    def relay(self, n):
        first = self.ORDER[n]
        for half in () if self.direct else range(2):
            self.arrived(half, self.block(half, first, 3, None), 4 + 4 * n)
            self.go(half, 1 - half, 1, self.block(half, first, 3, 0), 6 + 4 * n)
            self.arrived(half, self.block(half, first, 1, None), 5 + 4 * n)
            self.go(half, 1 - half, 3, self.block(half, first, 1, 1), 7 + 4 * n)

    def finish(self, half):
        for n in range(4):
            first = self.ORDER[n]
            if self.direct:
                self.arrived(half, self.block(half, first, 3, None), 4 + 4 * n)
                self.arrived(half, self.block(half, first, 1, None), 5 + 4 * n)
                self.arrived(half, self.block(half, first, 2, None), 6 + 4 * n)
            else:
                self.arrived(half, self.block(half, first, 2, 0), 6 + 4 * n)
                self.arrived(half, self.block(half, first, 2, 1), 7 + 4 * n)

    def drain(self):
        for copy in self.sent:
            copy.wait_send()


class Scatter:
    ORDER = (2, 1, 3, 0)

    def __init__(self, ring, part, base, rows, direct, far, near, last, out, send_sems, recv_sems):
        self.ring, self.part, self.base, self.direct, self.out = ring, part, base, direct, out
        self.far, self.near, self.last = far, near, last
        self.send_sems, self.recv_sems = send_sems, recv_sems
        self.n = rows // 2
        self.sent = []

    def block(self, half, first, second, lo, size):
        axis = 1 - half
        a, b = self.ring.along(axis, first), self.ring.along(1 - axis, second)
        y, x = (a, b) if axis == 1 else (b, a)
        return self.part.at[y, x, pl.ds(self.base + half * self.n + lo, size), :]

    def go(self, half, axis, step, src, dst, k):
        self.sent.append(
            send(
                src,
                dst,
                self.send_sems.at[half, k],
                self.recv_sems.at[half, k],
                self.ring.device(axis, step),
            )
        )

    def arrived(self, half, ref, k):
        pltpu.make_async_copy(ref, ref, self.recv_sems.at[half, k]).wait()

    def start(self, half):
        q = self.n // 2
        for m in range(4):
            o = self.ORDER[m]
            if self.direct:
                for way, step in ((0, 1), (1, 3)):
                    src = self.block(half, step, o, 0, self.n)
                    self.go(half, 1 - half, step, src, self.near.at[half, way, m], 4 * m + 2 + way)
                src = self.block(half, 2, o, 0, self.n)
                self.go(half, 1 - half, 2, src, self.far.at[half, m], 4 * m)
            else:
                for way, step in ((0, 1), (1, 3)):
                    src = self.block(half, 2, o, way * q, q)
                    dst = self.far.at[half, m, pl.ds(way * q, q), :]
                    self.go(half, 1 - half, step, src, dst, 4 * m + way)

    def pass_on(self, half, m):
        q, o = self.n // 2, self.ORDER[m]
        for way, step in () if self.direct else ((0, 1), (1, 3)):
            come = self.far.at[half, m, pl.ds(way * q, q), :]
            self.arrived(half, come, 4 * m + way)
            mine = self.block(half, step, o, way * q, q)
            mine[...] = (mine[...].astype(F32) + come[...].astype(F32)).astype(BF16)
            self.go(
                half,
                1 - half,
                step,
                self.block(half, step, o, 0, self.n),
                self.near.at[half, way, m],
                4 * m + 2 + way,
            )

    def collect(self, half, m):
        o = self.ORDER[m]
        for way in range(2):
            self.arrived(half, self.near.at[half, way, m], 4 * m + 2 + way)
        mine = self.block(half, 0, o, 0, self.n)
        total = mine[...].astype(F32) + self.near[half, 0, m].astype(F32)
        total = total + self.near[half, 1, m].astype(F32)
        if self.direct:
            self.arrived(half, self.far.at[half, m], 4 * m)
            total = total + self.far[half, m].astype(F32)
        mine[...] = total.astype(BF16)
        if m < 3:
            self.go(half, half, o, mine, self.last.at[half, m], 16 + m)

    def end(self, half):
        total = self.block(half, 0, 0, 0, self.n)[...].astype(F32)
        for m in (1, 2, 0):
            self.arrived(half, self.last.at[half, m], 16 + m)
            total = total + self.last[half, m].astype(F32)
        self.out[pl.ds(self.base + half * self.n, self.n), :] = total.astype(BF16)

    def drain(self):
        for copy in self.sent:
            copy.wait_send()


def kernel(
    ep_count,
    q_hbm,
    right_hbm,
    left_hbm,
    v_hbm,
    bounds_hbm,
    spikes_hbm,
    gain_hbm,
    emit_ref,
    rows_hbm,
    rows_gain_hbm,
    ids_hbm,
    shares_hbm,
    switch_ref,
    widen_ref,
    shrink_ref,
    out_a_ref,
    out_b_ref,
    q_ref,
    right_ref,
    left_ref,
    v_ref,
    bounds_ref,
    spikes_ref,
    gain_ref,
    rows_ref,
    rows_gain_ref,
    ids_ref,
    shares_ref,
    switch_buf,
    widen_buf,
    shrink_buf,
    emit_a,
    emit_b,
    outgoing,
    ebuf,
    part,
    far,
    near,
    last,
    expert_out,
    returned,
    picks,
    intra,
    query_f,
    query_b,
    added_f,
    added_b,
    chunk_decay,
    leg1_out,
    leg1_in,
    leg2_out,
    leg2_in,
    mixed_in,
    mixed_part,
    mixed_come,
    load_sems,
    all_send,
    all_recv,
    eg_send,
    eg_recv,
    m_send,
    m_recv,
    rs_send,
    rs_recv,
):
    z, c = lax.axis_index("z"), lax.axis_index("c")
    y, x = lax.axis_index("y"), lax.axis_index("x")
    s, t = 2 * z + c, 4 * y + x
    ring = Ring(z, c, y, x)
    tok = q_ref.shape[0]
    chunks = tok // CHUNK
    rows_b = rows_ref.shape[0]
    slots = ep_count * CAP
    near_count = ep_count // 2
    shift = ep_count // 4

    def ep_peer(k):
        other = lax.rem(s + k, ep_count)
        return other, (lax.div(other, 2), lax.rem(other, 2), y, x)

    columns = pl.ds(pl.multiple_of(t * LANES, LANES), LANES)

    def far_columns(_, to):
        return pl.ds(pl.multiple_of(to * (4 * LANES), 4 * LANES), 4 * LANES)

    def near_columns(k, to):
        return pl.ds(pl.multiple_of((4 * k + to) * LANES, LANES), LANES)

    def near_place(k):
        return pl.ds(k * LANES, LANES)

    core_rows = pl.ds(pl.multiple_of(c * (LANES // 2), LANES // 2), LANES // 2)
    loads = [
        pltpu.make_async_copy(src, dst, load_sems.at[i])
        for i, (src, dst) in enumerate(
            (
                (ids_hbm, ids_ref),
                (rows_hbm, rows_ref),
                (rows_gain_hbm, rows_gain_ref),
                (bounds_hbm, bounds_ref),
                (spikes_hbm, spikes_ref),
                (q_hbm, q_ref),
                (right_hbm, right_ref),
                (left_hbm, left_ref),
                (v_hbm, v_ref),
                (gain_hbm, gain_ref),
                (shares_hbm, shares_ref),
                (switch_ref.at[0], switch_buf),
                (widen_ref.at[0], widen_buf),
                (shrink_ref.at[0], shrink_buf),
                (emit_ref.at[core_rows, far_columns(0, y)], emit_b.at[y, core_rows, :]),
                *(
                    (emit_ref.at[core_rows, near_columns(k, x)], emit_a.at[x, core_rows, near_place(k)])
                    for k in range(4)
                ),
            )
        )
    ]
    for load in loads:
        load.start()
    barrier = pltpu.get_barrier_semaphore()

    def greet(k):
        pl.semaphore_signal(barrier, inc=1, device_id=ep_peer(k)[1], device_id_type=MESH)

    def greet_ep(k, _):
        greet(near_count - k)
        greet(near_count + k)
        return _

    greet(near_count)
    lax.fori_loop(1, near_count, greet_ep, 0)
    for axis in range(2):
        for step in range(1, 4):
            pl.semaphore_signal(
                barrier, inc=1, device_id=ring.device(axis, step), device_id_type=MESH
            )

    for load in loads[:3]:
        load.wait()

    width = rows_ref.shape[1]
    square = jnp.zeros((rows_b, LANES), F32)
    for k in range(width // LANES):
        piece = rows_ref[:, k * LANES : (k + 1) * LANES].astype(F32)
        square = square + piece * piece
    mean = jnp.sum(square, axis=1, keepdims=True) / width
    normed = rows_ref[:, columns].astype(F32) * lax.rsqrt(mean + EPS)
    normed = (normed * rows_gain_ref[:, columns]).astype(BF16)
    experts = iota((ep_count, rows_b), 0)
    pick0 = ids_ref[0:1, :] == experts
    pick1 = ids_ref[1:2, :] == experts
    named = (pick0 | pick1).astype(F32).astype(BF16)
    earlier = (iota((rows_b, rows_b), 0) < iota((rows_b, rows_b), 1)).astype(F32).astype(BF16)
    rank = nn(named, earlier)
    at_slot = rank.astype(jnp.int32)[:, None, :] == iota((ep_count, CAP, rows_b), 1)
    ones = jnp.where(at_slot, 1.0, 0.0)
    for k, pick in enumerate((pick0, pick1)):
        chosen = ones * jnp.where(pick, 1.0, 0.0)[:, None, :]
        picks[k] = chosen.reshape(slots, rows_b).astype(BF16)
    outgoing[...] = nn(picks[0] + picks[1], normed).astype(BF16)
    own_slots = pl.ds(pl.multiple_of(s * CAP, CAP), CAP)
    ebuf[y, x, shift * CAP : (shift + 1) * CAP, :] = outgoing[own_slots, :]

    pl.semaphore_wait(barrier, ep_count - 1 + 6)

    def dispatch(group):
        def one(k, _):
            other, device = ep_peer(k)
            place = lax.rem(shift - k + ep_count, ep_count)
            send(
                outgoing.at[pl.ds(pl.multiple_of(other * CAP, CAP), CAP), :],
                ebuf.at[y, x, pl.ds(pl.multiple_of(place * CAP, CAP), CAP), :],
                all_send.at[group],
                all_recv.at[group],
                device,
            )
            return _

        return one

    def leg1(k, _):
        other, device = ep_peer(k)
        send(
            leg1_out.at[lax.div(other, 2), lax.rem(other, 2)],
            leg1_in.at[s],
            all_send.at[2],
            all_recv.at[2],
            device,
        )
        return _

    def leg2(k, _):
        other, device = ep_peer(k)
        send(leg2_out.at[other], leg2_in.at[s], all_send.at[3], all_recv.at[3], device)
        return _

    def deal():
        for step in range(1, 4):
            for k in range(4):
                send(
                    emit_ref.at[core_rows, near_columns(k, ring.along(0, step))],
                    emit_a.at[x, core_rows, near_place(k)],
                    all_send.at[4],
                    all_recv.at[4],
                    ring.device(0, step),
                )
            send(
                emit_ref.at[core_rows, far_columns(0, ring.along(1, step))],
                emit_b.at[y, core_rows, :],
                all_send.at[7],
                all_recv.at[7],
                ring.device(1, step),
            )

    def give_back(k, _):
        other, device = ep_peer(k)
        place = lax.rem(shift + k, ep_count)
        send(
            expert_out.at[pl.ds(pl.multiple_of(place * CAP, CAP), CAP), :],
            returned.at[own_slots, :],
            all_send.at[5],
            all_recv.at[5],
            device,
        )
        return _

    def all_arrived(ref, k):
        pltpu.make_async_copy(ref, ref, all_recv.at[k]).wait()

    def all_sent(ref, k):
        pltpu.make_async_copy(ref, ref, all_send.at[k]).wait()

    near_slots = outgoing.at[pl.ds(0, (near_count - 1) * CAP), :]
    far_slots = outgoing.at[pl.ds(0, near_count * CAP), :]
    others_slots = outgoing.at[pl.ds(0, slots - CAP), :]
    rows = slots // 2
    gather = [Gather(ring, ebuf, p * rows, rows, DIRECT_GATHER[p], eg_send.at[p], eg_recv.at[p]) for p in range(2)]
    scatter = [
        Scatter(
            ring,
            part,
            p * rows,
            rows,
            DIRECT_SCATTER[p],
            far.at[p],
            near.at[p],
            last.at[p],
            expert_out,
            rs_send.at[p],
            rs_recv.at[p],
        )
        for p in range(2)
    ]

    def experts_of(p):
        at = pl.ds(p * rows, rows)
        tokens = jnp.concatenate([ebuf[k // 4, k % 4, at, :] for k in range(16)], axis=1)
        opened = nt(tokens, switch_buf[...])
        opened = opened * jax.nn.sigmoid(opened)
        hidden = (opened * nt(tokens, widen_buf[...])).astype(BF16)
        for k in range(4):
            product = nn(hidden, shrink_buf[:, k * 512 : (k + 1) * 512]).astype(BF16)
            for m in range(4):
                part[k, m, at, :] = product[:, m * LANES : (m + 1) * LANES]

    lax.fori_loop(1, shift + 1, dispatch(0), 0)
    lax.fori_loop(ep_count - shift + 1, ep_count, dispatch(0), 0)
    lax.fori_loop(shift + 1, ep_count - shift + 1, dispatch(1), 0)
    deal()

    for load in loads[3:9]:
        load.wait()
    tri = iota((CHUNK, CHUNK), 0) >= iota((CHUNK, CHUNK), 1)
    tri_t = iota((CHUNK, CHUNK), 0) <= iota((CHUNK, CHUNK), 1)
    for n in range(chunks):
        at = slice(n * CHUNK, (n + 1) * CHUNK)
        query = q_ref[at, :].astype(F32)
        query = query * jax.nn.sigmoid(query)
        values = v_ref[at, :]
        spike = spikes_ref[0:1, at]
        scores = []
        for d, (pre_ref, mask, queries, added) in enumerate(
            ((right_ref, tri, query_f, added_f), (left_ref, tri_t, query_b, added_b))
        ):
            pre = pre_ref[at, :].astype(F32)
            bound = bounds_ref[d : d + 1, :]
            gap = 1.0 - bound
            log_decay = jnp.log(bound + gap * jax.nn.sigmoid(pre))
            key = gap * jax.nn.sigmoid(-pre)
            split = jnp.concatenate(three_parts(log_decay), axis=1).astype(BF16)
            summed = nn(jnp.where(mask, 1.0, 0.0).astype(BF16), split)
            total = summed[:, :LANES] + summed[:, LANES : 2 * LANES] + summed[:, 2 * LANES :]
            total = total + jnp.sum(jnp.where(mask, spike, 0.0), axis=1, keepdims=True)
            whole = total[CHUNK - 1 : CHUNK, :] if d == 0 else total[0:1, :]
            middle = total[CHUNK // 2 : CHUNK // 2 + 1, :]
            near_q = (query * jnp.exp(total - middle)).astype(BF16)
            near_k = (key * jnp.exp(middle - total)).astype(BF16)
            scores.append(jnp.where(mask, nt(near_q, near_k), 0.0))
            queries[at, :] = (query * jnp.exp(total)).astype(BF16)
            added[n] = tn(values, (key * jnp.exp(whole - total)).astype(BF16))
            chunk_decay[d, n] = whole
        intra[at, :] = nn((scores[0] + scores[1]).astype(BF16), values)

    z_count = ep_count // 2
    rows_s = LANES // z_count
    for d, (added, order) in enumerate(
        ((added_f, range(chunks)), (added_b, range(chunks - 1, -1, -1)))
    ):
        state, decay = None, None
        for n in order:
            state = added[n] if state is None else state * jnp.exp(chunk_decay[d, n]) + added[n]
            decay = chunk_decay[d, n] if decay is None else decay + chunk_decay[d, n]
        hi, mid, lo = three_parts(decay)
        row = iota((8, LANES), 0)
        tail = jnp.where(row == 0, hi, jnp.where(row == 1, mid, jnp.where(row == 2, lo, 0.0)))
        tail = jnp.broadcast_to(tail[None], (z_count, 8, LANES))
        leg1_out[:, d] = jnp.concatenate(
            [state.reshape(z_count, rows_s, LANES), tail], axis=1
        ).astype(BF16)
    leg1_in[s] = leg1_out[z, c]
    all_arrived(near_slots, 0)
    gather[0].start()
    gather[0].near()
    gather[0].far()
    lax.fori_loop(1, ep_count, leg1, 0)
    gather[0].relay(0)
    all_arrived(far_slots, 1)
    gather[1].start()
    gather[0].relay(1)
    gather[0].relay(2)
    gather[0].relay(3)
    gather[1].near()
    gather[1].far()
    gather[1].relay(0)
    gather[1].relay(1)
    gather[1].relay(2)
    gather[1].relay(3)
    for load in loads[14:19]:
        load.wait()
    dealt = emit_a.at[pl.ds(0, 3), pl.ds(0, LANES // 2), :]
    all_arrived(dealt, 4)
    all_arrived(dealt, 7)
    for emit, k in ((emit_a, 6), (emit_b, 8)):
        block = emit.at[:, core_rows, :]
        send(block, block, all_send.at[k], all_recv.at[k], (z, 1 - c, y, x))
    all_arrived(leg1_in.at[pl.ds(0, ep_count - 1)], 2)
    carried = jnp.zeros((rows_s, LANES), F32)
    for n in range(ep_count):
        i = jnp.where(c == 0, n, ep_count - 1 - n)
        tile = leg1_in[i].astype(F32)
        leg2_out[i] = carried.astype(BF16)
        decay = tile[rows_s : rows_s + 1] + tile[rows_s + 1 : rows_s + 2] + tile[rows_s + 2 : rows_s + 3]
        carried = carried * jnp.exp(decay) + tile[:rows_s]
    lax.fori_loop(1, ep_count, leg2, 0)
    leg2_in[s] = leg2_out[s]
    for half in range(2):
        gather[0].finish(half)
    for load in loads[11:14]:
        load.wait()
    experts_of(0)
    for half in range(2):
        scatter[0].start(half)
    for half in range(2):
        gather[1].finish(half)
    experts_of(1)
    for half in range(2):
        scatter[1].start(half)
    for m in range(4):
        for half in range(2):
            scatter[0].pass_on(half, m)
    for m in range(4):
        for half in range(2):
            scatter[1].pass_on(half, m)
    for m in range(4):
        for half in range(2):
            scatter[0].collect(half, m)
    all_arrived(leg2_in.at[pl.ds(0, ep_count - 1)], 3)
    loads[9].wait()
    entries = [
        jnp.concatenate([leg2_in[2 * k + d].astype(F32) for k in range(z_count)], axis=0)
        for d in range(2)
    ]
    for d, (added, queries, order) in enumerate(
        ((added_f, query_f, range(chunks)), (added_b, query_b, range(chunks - 1, -1, -1)))
    ):
        state = entries[d]
        for n in order:
            at = slice(n * CHUNK, (n + 1) * CHUNK)
            intra[at, :] += nt(queries[at, :], state.astype(BF16))
            state = state * jnp.exp(chunk_decay[d, n]) + added[n]
    mixed = intra[...]
    mixed = mixed * lax.rsqrt(jnp.mean(mixed * mixed, axis=1, keepdims=True) + EPS)
    mixed = (mixed * gain_ref[...]).astype(BF16)
    mixed_in[0, x] = mixed[: tok // 2]
    mixed_in[1, y] = mixed[tok // 2 :]
    flows_m = []
    for half in range(2):
        own = mixed_in.at[half, (x, y)[half]]
        for step in range(1, 4):
            flows_m.append(
                send(own, own, m_send.at[0, half, step], m_recv.at[0, half, step], ring.device(half, step))
            )
    for m in range(4):
        for half in range(2):
            scatter[1].collect(half, m)
    for half in range(2):
        scatter[0].end(half)
    lax.fori_loop(1, near_count - shift, give_back, 0)
    lax.fori_loop(ep_count - shift, ep_count, give_back, 0)
    returned[own_slots, :] = expert_out[shift * CAP : (shift + 1) * CAP, :]
    for half in range(2):
        scatter[1].end(half)
    lax.fori_loop(near_count - shift, ep_count - shift, give_back, 0)
    whole = emit_a.at[:, pl.ds(0, LANES // 2), :]
    all_arrived(whole, 6)
    all_arrived(whole, 8)
    for half in range(2):
        for step in range(1, 4):
            come = mixed_in.at[half, ring.along(half, step)]
            pltpu.make_async_copy(come, come, m_recv.at[0, half, step]).wait()
        heads = jnp.concatenate([mixed_in[half, k] for k in range(4)], axis=1)
        emit = (emit_a, emit_b)[half][...].reshape(4 * LANES, 4 * LANES)
        product = nn(heads, emit)
        for k in range(4):
            mixed_part[half, k] = product[:, k * LANES : (k + 1) * LANES].astype(BF16)
        for step in range(1, 4):
            flows_m.append(
                send(
                    mixed_part.at[half, ring.along(1 - half, step)],
                    mixed_come.at[half, step],
                    m_send.at[1, half, step],
                    m_recv.at[1, half, step],
                    ring.device(1 - half, step),
                )
            )
    for half in range(2):
        total = mixed_part[half, (y, x)[half]].astype(F32)
        for step in range(1, 4):
            come = mixed_come.at[half, step]
            pltpu.make_async_copy(come, come, m_recv.at[1, half, step]).wait()
            total = total + mixed_come[half, step].astype(F32)
        out_a_ref[half * (tok // 2) : (half + 1) * (tok // 2), :] = total.astype(BF16)
    all_arrived(others_slots, 5)
    loads[10].wait()
    results = returned[...]
    same = iota((rows_b, rows_b), 0) == iota((rows_b, rows_b), 1)
    mixed_b = jnp.zeros((rows_b, LANES), F32)
    for k in range(2):
        share = jnp.sum(jnp.where(same, shares_ref[k : k + 1, :], 0.0), axis=1, keepdims=True)
        mixed_b = mixed_b + tn(picks[k], results) * share
    out_b_ref[...] = mixed_b.astype(BF16)

    all_sent(near_slots, 0)
    all_sent(far_slots, 1)
    all_sent(leg1_in.at[pl.ds(0, ep_count - 1)], 2)
    all_sent(leg2_in.at[pl.ds(0, ep_count - 1)], 3)
    for k in (4, 7):
        all_sent(dealt, k)
    for k in (6, 8):
        all_sent(whole, k)
    for copy in flows_m:
        copy.wait_send()
    all_sent(others_slots, 5)
    for flow in (*gather, *scatter):
        flow.drain()


def per_device(*args):
    (q, right, left, v, bounds, spikes, gain, emit, rows, rows_gain, ids, shares, switch, widen, shrink) = args
    ep_count = lax.axis_size("z") * 2
    tok, rows_b, width = q.shape[0], rows.shape[0], rows.shape[1]
    hidden = switch.shape[2]
    slots = ep_count * CAP
    chunks = tok // CHUNK
    z_count = ep_count // 2
    rows_s = LANES // z_count
    n = slots // 4
    dma = pltpu.SemaphoreType.DMA
    return pl.pallas_call(
        functools.partial(kernel, ep_count),
        out_shape=(
            pltpu.VMEM((tok, LANES), BF16),
            pltpu.VMEM((rows_b, LANES), BF16),
        ),
        in_specs=[pl.BlockSpec(memory_space=pl.ANY)] * 15,
        out_specs=(pl.BlockSpec(memory_space=pltpu.VMEM),) * 2,
        scratch_shapes=[
            pltpu.VMEM((tok, LANES), BF16),
            pltpu.VMEM((tok, LANES), BF16),
            pltpu.VMEM((tok, LANES), BF16),
            pltpu.VMEM((tok, LANES), BF16),
            pltpu.VMEM((2, LANES), F32),
            pltpu.VMEM((1, tok), F32),
            pltpu.VMEM((1, LANES), F32),
            pltpu.VMEM((rows_b, width), BF16),
            pltpu.VMEM((1, width), F32),
            pltpu.VMEM((2, rows_b), jnp.int32),
            pltpu.VMEM((2, rows_b), F32),
            pltpu.VMEM((hidden, width), BF16),
            pltpu.VMEM((hidden, width), BF16),
            pltpu.VMEM((hidden, width), BF16),
            pltpu.VMEM((4, LANES, 4 * LANES), BF16),
            pltpu.VMEM((4, LANES, 4 * LANES), BF16),
            pltpu.VMEM((slots, LANES), BF16),
            pltpu.VMEM((4, 4, slots, LANES), BF16),
            pltpu.VMEM((4, 4, slots, LANES), BF16),
            pltpu.VMEM((2, 2, 4, n, LANES), BF16),
            pltpu.VMEM((2, 2, 2, 4, n, LANES), BF16),
            pltpu.VMEM((2, 2, 3, n, LANES), BF16),
            pltpu.VMEM((slots, LANES), BF16),
            pltpu.VMEM((slots, LANES), BF16),
            pltpu.VMEM((2, slots, rows_b), BF16),
            pltpu.VMEM((tok, LANES), F32),
            pltpu.VMEM((tok, LANES), BF16),
            pltpu.VMEM((tok, LANES), BF16),
            pltpu.VMEM((chunks, LANES, LANES), F32),
            pltpu.VMEM((chunks, LANES, LANES), F32),
            pltpu.VMEM((2, chunks, 1, LANES), F32),
            pltpu.VMEM((z_count, 2, rows_s + 8, LANES), BF16),
            pltpu.VMEM((ep_count, rows_s + 8, LANES), BF16),
            pltpu.VMEM((ep_count, rows_s, LANES), BF16),
            pltpu.VMEM((ep_count, rows_s, LANES), BF16),
            pltpu.VMEM((2, 4, tok // 2, LANES), BF16),
            pltpu.VMEM((2, 4, tok // 2, LANES), BF16),
            pltpu.VMEM((2, 4, tok // 2, LANES), BF16),
            dma((19,)),
            dma((9,)),
            dma((9,)),
            dma((2, 2, 20)),
            dma((2, 2, 20)),
            dma((2, 2, 4)),
            dma((2, 2, 4)),
            dma((2, 2, 20)),
            dma((2, 2, 20)),
        ],
        compiler_params=pltpu.CompilerParams(collective_id=0, has_side_effects=True),
    )(
        q,
        right,
        left,
        v,
        bounds,
        spikes,
        gain.reshape(1, -1),
        emit,
        rows,
        rows_gain.reshape(1, -1),
        ids.T,
        shares.T,
        switch.transpose(0, 2, 1),
        widen.transpose(0, 2, 1),
        shrink,
    )


def solution(mesh):
    ep, tp = mesh.shape["ep"], mesh.shape["tp"]
    split = Mesh(mesh.devices.reshape(ep // 2, 2, tp // 4, 4), ("z", "c", "y", "x"))
    e, f = ("z", "c"), ("y", "x")
    return jax.shard_map(
        per_device,
        mesh=split,
        in_specs=(
            P(e, f),
            P(e, f),
            P(e, f),
            P(e, f),
            P(None, f),
            P(f, e),
            P(f),
            P(f, None),
            P(e, None),
            P(),
            P(e, None),
            P(e, None),
            P(e, None, f),
            P(e, None, f),
            P(e, f, None),
        ),
        out_specs=(P(e, f), P(e, f)),
        check_vma=False,
    )
```

time: 89.5 us -> 70 us (0.78)
  Pallas kernels: 86.5 us -> 68 us
  local copies, waits for them, and re-layouts: 2.19 us -> 1.27 us
    pallas_call x1, Pallas kernels: 86.5 us -> 68 us  [per_device(): pl.pallas_call(functools.partial(kernel, ep_count), out_shape=(pltpu.VMEM...]
    unnamed x4 -> x2, local copies, waits for them, and re-layouts: 2.19 us -> 1.27 us
where the time goes in v2:
time: 70 us; the launch traced here: 69.9 us
  Pallas kernels  68 us (97%)
  local copies, waits for them, and re-layouts  1.27 us (2%)
    pallas_call x1, Pallas kernels, per_device(): pl.pallas_call(functools.partial(kernel, ep_count), out_shape=(pltpu.VMEM...  68 us

profile of v2, /device:TPU:1, one launch (start us, length us, event | category | flops | bytes accessed | tf_op | source)
XLA Modules:
  0.0 69.9 jit_solution(18084782892322088571)
XLA Ops:
  0.6 68.0 %shard_map.158 = (bf16[512,128]{1,0:T(8,128)(2,1)S(1)}, bf16[128,128]{1,0:T(8,128)(2,1)S(1)}) custom-call(bf16[512,128]{1,0:T(8,128)(2,1)} %q_hbm.1, bf16[512,128]{1,0:T(8,128)(2,1)} %right_hbm.1, bf16[512,128]{1,0:T(8,128)(2,1)} %left_hbm.1, bf16[512,128]{1,0:T(8,128)(2,1)} %v_hbm.1, f32[2,128]{1,0:T(2,128)} %bounds_hbm.1, f32[1,512]{1,0:T(1,128)} %spikes_hbm.1, ...), custom_call_target="tpu_custom_call" | custom-call | tf_op jit(solution)/shard_map/pallas_call | solution.py:721
  68.6 0.7 copy.19
  69.3 0.6 copy.20

commit v3 on v2

--- a/solution.py
+++ b/solution.py
@@ -281,6 +281,8 @@
     expert_out,
     returned,
     picks,
+    taken,
+    share_columns,
     intra,
     query_f,
     query_b,
@@ -364,13 +366,19 @@
     def greet(k):
         pl.semaphore_signal(barrier, inc=1, device_id=ep_peer(k)[1], device_id_type=MESH)
 
-    def greet_ep(k, _):
-        greet(near_count - k)
-        greet(near_count + k)
-        return _
-
-    greet(near_count)
-    lax.fori_loop(1, near_count, greet_ep, 0)
+    def pairs(one, low, high, count):
+        def both(i, _):
+            one(low - i)
+            one(high + i)
+            return _
+
+        lax.fori_loop(0, count, both, 0)
+
+    def everyone(one):
+        one(near_count)
+        pairs(one, near_count - 1, near_count + 1, near_count - 1)
+
+    everyone(greet)
     for axis in range(2):
         for step in range(1, 4):
             pl.semaphore_signal(
@@ -406,7 +414,7 @@
     pl.semaphore_wait(barrier, ep_count - 1 + 6)
 
     def dispatch(group):
-        def one(k, _):
+        def one(k):
             other, device = ep_peer(k)
             place = lax.rem(shift - k + ep_count, ep_count)
             send(
@@ -416,11 +424,10 @@
                 all_recv.at[group],
                 device,
             )
-            return _
 
         return one
 
-    def leg1(k, _):
+    def leg1(k):
         other, device = ep_peer(k)
         send(
             leg1_out.at[lax.div(other, 2), lax.rem(other, 2)],
@@ -429,12 +436,10 @@
             all_recv.at[2],
             device,
         )
-        return _
-
-    def leg2(k, _):
+
+    def leg2(k):
         other, device = ep_peer(k)
         send(leg2_out.at[other], leg2_in.at[s], all_send.at[3], all_recv.at[3], device)
-        return _
 
     def deal():
         for step in range(1, 4):
@@ -454,7 +459,7 @@
                 ring.device(1, step),
             )
 
-    def give_back(k, _):
+    def give_back(k):
         other, device = ep_peer(k)
         place = lax.rem(shift + k, ep_count)
         send(
@@ -464,7 +469,6 @@
             all_recv.at[5],
             device,
         )
-        return _
 
     def all_arrived(ref, k):
         pltpu.make_async_copy(ref, ref, all_recv.at[k]).wait()
@@ -505,9 +509,9 @@
             for m in range(4):
                 part[k, m, at, :] = product[:, m * LANES : (m + 1) * LANES]
 
-    lax.fori_loop(1, shift + 1, dispatch(0), 0)
-    lax.fori_loop(ep_count - shift + 1, ep_count, dispatch(0), 0)
-    lax.fori_loop(shift + 1, ep_count - shift + 1, dispatch(1), 0)
+    for low, high in ((1, shift + 1), (ep_count - shift + 1, ep_count)):
+        lax.fori_loop(low, high, lambda k, _: dispatch(0)(k), None)
+    pairs(dispatch(1), near_count, near_count + 1, near_count - shift)
     deal()
 
     for load in loads[3:9]:
@@ -564,7 +568,13 @@
     gather[0].start()
     gather[0].near()
     gather[0].far()
-    lax.fori_loop(1, ep_count, leg1, 0)
+    loads[10].wait()
+    same = iota((rows_b, rows_b), 0) == iota((rows_b, rows_b), 1)
+    for k in range(2):
+        taken[k] = picks[k].T
+        share = jnp.sum(jnp.where(same, shares_ref[k : k + 1, :], 0.0), axis=1, keepdims=True)
+        share_columns[k] = jnp.broadcast_to(share, (rows_b, LANES))
+    everyone(leg1)
     gather[0].relay(0)
     all_arrived(far_slots, 1)
     gather[1].start()
@@ -585,6 +595,13 @@
     for emit, k in ((emit_a, 6), (emit_b, 8)):
         block = emit.at[:, core_rows, :]
         send(block, block, all_send.at[k], all_recv.at[k], (z, 1 - c, y, x))
+    for half in range(2):
+        gather[0].finish(half)
+    for load in loads[11:14]:
+        load.wait()
+    experts_of(0)
+    for half in range(2):
+        scatter[0].start(half)
     all_arrived(leg1_in.at[pl.ds(0, ep_count - 1)], 2)
     carried = jnp.zeros((rows_s, LANES), F32)
     for n in range(ep_count):
@@ -593,15 +610,8 @@
         leg2_out[i] = carried.astype(BF16)
         decay = tile[rows_s : rows_s + 1] + tile[rows_s + 1 : rows_s + 2] + tile[rows_s + 2 : rows_s + 3]
         carried = carried * jnp.exp(decay) + tile[:rows_s]
-    lax.fori_loop(1, ep_count, leg2, 0)
+    everyone(leg2)
     leg2_in[s] = leg2_out[s]
-    for half in range(2):
-        gather[0].finish(half)
-    for load in loads[11:14]:
-        load.wait()
-    experts_of(0)
-    for half in range(2):
-        scatter[0].start(half)
     for half in range(2):
         gather[1].finish(half)
     experts_of(1)
@@ -616,6 +626,9 @@
     for m in range(4):
         for half in range(2):
             scatter[0].collect(half, m)
+    for m in range(4):
+        for half in range(2):
+            scatter[1].collect(half, m)
     all_arrived(leg2_in.at[pl.ds(0, ep_count - 1)], 3)
     loads[9].wait()
     entries = [
@@ -633,65 +646,82 @@
     mixed = intra[...]
     mixed = mixed * lax.rsqrt(jnp.mean(mixed * mixed, axis=1, keepdims=True) + EPS)
     mixed = (mixed * gain_ref[...]).astype(BF16)
-    mixed_in[0, x] = mixed[: tok // 2]
-    mixed_in[1, y] = mixed[tok // 2 :]
+    mixed = mixed.reshape(2, 2, tok // 4, LANES)
+    mixed_in[0, x] = mixed[0]
+    mixed_in[1, y] = mixed[1]
+    def flow_m(stage, half, part_m, step, src, dst, axis):
+        return pltpu.make_async_remote_copy(
+            src_ref=src,
+            dst_ref=dst,
+            send_sem=m_send.at[stage, half, part_m, step],
+            recv_sem=m_recv.at[stage, half, part_m, step],
+            device_id=ring.device(axis, step),
+            device_id_type=MESH,
+        )
+
     flows_m = []
-    for half in range(2):
-        own = mixed_in.at[half, (x, y)[half]]
-        for step in range(1, 4):
-            flows_m.append(
-                send(own, own, m_send.at[0, half, step], m_recv.at[0, half, step], ring.device(half, step))
-            )
-    for m in range(4):
-        for half in range(2):
-            scatter[1].collect(half, m)
+    for part_m in range(2):
+        for half in range(2):
+            own = mixed_in.at[half, (x, y)[half], part_m]
+            for step in range(1, 4):
+                flows_m.append(flow_m(0, half, part_m, step, own, own, half))
+
+    def heads_out(core):
+        @pl.when(c == core)
+        def _():
+            for flow in flows_m[:12]:
+                flow.start()
+
+    heads_out(0)
     for half in range(2):
         scatter[0].end(half)
-    lax.fori_loop(1, near_count - shift, give_back, 0)
-    lax.fori_loop(ep_count - shift, ep_count, give_back, 0)
+    pairs(give_back, shift - 1, ep_count - shift, shift - 1)
+    give_back(ep_count - 1)
     returned[own_slots, :] = expert_out[shift * CAP : (shift + 1) * CAP, :]
     for half in range(2):
         scatter[1].end(half)
-    lax.fori_loop(near_count - shift, ep_count - shift, give_back, 0)
+    give_back(near_count)
+    pairs(give_back, near_count - 1, near_count + 1, near_count - shift - 1)
+    give_back(shift)
+    heads_out(1)
     whole = emit_a.at[:, pl.ds(0, LANES // 2), :]
     all_arrived(whole, 6)
     all_arrived(whole, 8)
-    for half in range(2):
-        for step in range(1, 4):
-            come = mixed_in.at[half, ring.along(half, step)]
-            pltpu.make_async_copy(come, come, m_recv.at[0, half, step]).wait()
-        heads = jnp.concatenate([mixed_in[half, k] for k in range(4)], axis=1)
-        emit = (emit_a, emit_b)[half][...].reshape(4 * LANES, 4 * LANES)
-        product = nn(heads, emit)
-        for k in range(4):
-            mixed_part[half, k] = product[:, k * LANES : (k + 1) * LANES].astype(BF16)
-        for step in range(1, 4):
-            flows_m.append(
-                send(
-                    mixed_part.at[half, ring.along(1 - half, step)],
-                    mixed_come.at[half, step],
-                    m_send.at[1, half, step],
-                    m_recv.at[1, half, step],
-                    ring.device(1 - half, step),
+
+    def heads_in(part_m):
+        for half in range(2):
+            for step in range(1, 4):
+                come = mixed_in.at[half, ring.along(half, step), part_m]
+                pltpu.make_async_copy(come, come, m_recv.at[0, half, part_m, step]).wait()
+            heads = jnp.concatenate([mixed_in[half, k, part_m] for k in range(4)], axis=1)
+            emit = (emit_a, emit_b)[half][...].reshape(4 * LANES, 4 * LANES)
+            product = nn(heads, emit)
+            for k in range(4):
+                mixed_part[half, k, part_m] = product[:, k * LANES : (k + 1) * LANES].astype(BF16)
+            for step in range(1, 4):
+                flow = flow_m(
+                    1,
+                    half,
+                    part_m,
+                    step,
+                    mixed_part.at[half, ring.along(1 - half, step), part_m],
+                    mixed_come.at[half, step, part_m],
+                    1 - half,
                 )
-            )
-    for half in range(2):
-        total = mixed_part[half, (y, x)[half]].astype(F32)
-        for step in range(1, 4):
-            come = mixed_come.at[half, step]
-            pltpu.make_async_copy(come, come, m_recv.at[1, half, step]).wait()
-            total = total + mixed_come[half, step].astype(F32)
-        out_a_ref[half * (tok // 2) : (half + 1) * (tok // 2), :] = total.astype(BF16)
-    all_arrived(others_slots, 5)
-    loads[10].wait()
-    results = returned[...]
-    same = iota((rows_b, rows_b), 0) == iota((rows_b, rows_b), 1)
-    mixed_b = jnp.zeros((rows_b, LANES), F32)
-    for k in range(2):
-        share = jnp.sum(jnp.where(same, shares_ref[k : k + 1, :], 0.0), axis=1, keepdims=True)
-        mixed_b = mixed_b + tn(picks[k], results) * share
-    out_b_ref[...] = mixed_b.astype(BF16)
-
+                flow.start()
+                flows_m.append(flow)
+
+    heads_in(0)
+    heads_in(1)
+    for part_m in range(2):
+        for half in range(2):
+            total = mixed_part[half, (y, x)[half], part_m].astype(F32)
+            for step in range(1, 4):
+                come = mixed_come.at[half, step, part_m]
+                pltpu.make_async_copy(come, come, m_recv.at[1, half, part_m, step]).wait()
+                total = total + mixed_come[half, step, part_m].astype(F32)
+            start = (2 * half + part_m) * (tok // 4)
+            out_a_ref[start : start + tok // 4, :] = total.astype(BF16)
     all_sent(near_slots, 0)
     all_sent(far_slots, 1)
     all_sent(leg1_in.at[pl.ds(0, ep_count - 1)], 2)
@@ -702,9 +732,15 @@
         all_sent(whole, k)
     for copy in flows_m:
         copy.wait_send()
-    all_sent(others_slots, 5)
     for flow in (*gather, *scatter):
         flow.drain()
+    all_arrived(others_slots, 5)
+    all_sent(others_slots, 5)
+    results = returned[...]
+    mixed_b = jnp.zeros((rows_b, LANES), F32)
+    for k in range(2):
+        mixed_b = mixed_b + nn(taken[k], results) * share_columns[k]
+    out_b_ref[...] = mixed_b.astype(BF16)
 
 
 def per_device(*args):
@@ -752,6 +788,8 @@
             pltpu.VMEM((slots, LANES), BF16),
             pltpu.VMEM((slots, LANES), BF16),
             pltpu.VMEM((2, slots, rows_b), BF16),
+            pltpu.VMEM((2, rows_b, slots), BF16),
+            pltpu.VMEM((2, rows_b, LANES), F32),
             pltpu.VMEM((tok, LANES), F32),
             pltpu.VMEM((tok, LANES), BF16),
             pltpu.VMEM((tok, LANES), BF16),
@@ -762,16 +800,16 @@
             pltpu.VMEM((ep_count, rows_s + 8, LANES), BF16),
             pltpu.VMEM((ep_count, rows_s, LANES), BF16),
             pltpu.VMEM((ep_count, rows_s, LANES), BF16),
-            pltpu.VMEM((2, 4, tok // 2, LANES), BF16),
-            pltpu.VMEM((2, 4, tok // 2, LANES), BF16),
-            pltpu.VMEM((2, 4, tok // 2, LANES), BF16),
+            pltpu.VMEM((2, 4, 2, tok // 4, LANES), BF16),
+            pltpu.VMEM((2, 4, 2, tok // 4, LANES), BF16),
+            pltpu.VMEM((2, 4, 2, tok // 4, LANES), BF16),
             dma((19,)),
             dma((9,)),
             dma((9,)),
             dma((2, 2, 20)),
             dma((2, 2, 20)),
-            dma((2, 2, 4)),
-            dma((2, 2, 4)),
+            dma((2, 2, 2, 4)),
+            dma((2, 2, 2, 4)),
             dma((2, 2, 20)),
             dma((2, 2, 20)),
         ],

time: 70 us -> 68.4 us (0.977)
  Pallas kernels: 68 us -> 66.4 us
    pallas_call x1, Pallas kernels: 68 us -> 66.4 us  [per_device(): pl.pallas_call(functools.partial(kernel, ep_count), out_shape=(pltpu.VMEM...]
where the time goes in v3:
time: 68.4 us; the launch traced here: 68.3 us
  Pallas kernels  66.4 us (97%)
  local copies, waits for them, and re-layouts  1.27 us (2%)
    pallas_call x1, Pallas kernels, per_device(): pl.pallas_call(functools.partial(kernel, ep_count), out_shape=(pltpu.VMEM...  66.4 us

profile of v3, /device:TPU:1, one launch (start us, length us, event | category | flops | bytes accessed | tf_op | source)
XLA Modules:
  0.0 68.3 jit_solution(6935788855869151509)
XLA Ops:
  0.6 66.4 %shard_map.158 = (bf16[512,128]{1,0:T(8,128)(2,1)S(1)}, bf16[128,128]{1,0:T(8,128)(2,1)S(1)}) custom-call(bf16[512,128]{1,0:T(8,128)(2,1)} %q_hbm.1, bf16[512,128]{1,0:T(8,128)(2,1)} %right_hbm.1, bf16[512,128]{1,0:T(8,128)(2,1)} %left_hbm.1, bf16[512,128]{1,0:T(8,128)(2,1)} %v_hbm.1, f32[2,128]{1,0:T(2,128)} %bounds_hbm.1, f32[1,512]{1,0:T(1,128)} %spikes_hbm.1, ...), custom_call_target="tpu_custom_call" | custom-call | tf_op jit(solution)/shard_map/pallas_call | solution.py:757
  67.0 0.7 copy.19
  67.7 0.6 copy.20

commit v4 on v3

--- a/solution.py
+++ b/solution.py
@@ -619,16 +619,16 @@
         scatter[1].start(half)
     for m in range(4):
         for half in range(2):
+            scatter[1].pass_on(half, m)
+    for m in range(4):
+        for half in range(2):
             scatter[0].pass_on(half, m)
     for m in range(4):
         for half in range(2):
-            scatter[1].pass_on(half, m)
+            scatter[1].collect(half, m)
     for m in range(4):
         for half in range(2):
             scatter[0].collect(half, m)
-    for m in range(4):
-        for half in range(2):
-            scatter[1].collect(half, m)
     all_arrived(leg2_in.at[pl.ds(0, ep_count - 1)], 3)
     loads[9].wait()
     entries = [
@@ -674,15 +674,15 @@
 
     heads_out(0)
     for half in range(2):
+        scatter[1].end(half)
+    give_back(near_count)
+    pairs(give_back, near_count - 1, near_count + 1, near_count - shift - 1)
+    give_back(shift)
+    for half in range(2):
         scatter[0].end(half)
     pairs(give_back, shift - 1, ep_count - shift, shift - 1)
     give_back(ep_count - 1)
     returned[own_slots, :] = expert_out[shift * CAP : (shift + 1) * CAP, :]
-    for half in range(2):
-        scatter[1].end(half)
-    give_back(near_count)
-    pairs(give_back, near_count - 1, near_count + 1, near_count - shift - 1)
-    give_back(shift)
     heads_out(1)
     whole = emit_a.at[:, pl.ds(0, LANES // 2), :]
     all_arrived(whole, 6)

time: 68.4 us -> 67.5 us (0.987)
  Pallas kernels: 66.4 us -> 65.5 us
    pallas_call x1, Pallas kernels: 66.4 us -> 65.5 us  [per_device(): pl.pallas_call(functools.partial(kernel, ep_count), out_shape=(pltpu.VMEM...]
where the time goes in v4:
time: 67.5 us; the launch traced here: 67.4 us
  Pallas kernels  65.5 us (97%)
  local copies, waits for them, and re-layouts  1.27 us (2%)
    pallas_call x1, Pallas kernels, per_device(): pl.pallas_call(functools.partial(kernel, ep_count), out_shape=(pltpu.VMEM...  65.5 us

profile of v4, /device:TPU:1, one launch (start us, length us, event | category | flops | bytes accessed | tf_op | source)
XLA Modules:
  0.0 67.4 jit_solution(17684291073622462095)
XLA Ops:
  0.6 65.5 %shard_map.158 = (bf16[512,128]{1,0:T(8,128)(2,1)S(1)}, bf16[128,128]{1,0:T(8,128)(2,1)S(1)}) custom-call(bf16[512,128]{1,0:T(8,128)(2,1)} %q_hbm.1, bf16[512,128]{1,0:T(8,128)(2,1)} %right_hbm.1, bf16[512,128]{1,0:T(8,128)(2,1)} %left_hbm.1, bf16[512,128]{1,0:T(8,128)(2,1)} %v_hbm.1, f32[2,128]{1,0:T(2,128)} %bounds_hbm.1, f32[1,512]{1,0:T(1,128)} %spikes_hbm.1, ...), custom_call_target="tpu_custom_call" | custom-call | tf_op jit(solution)/shard_map/pallas_call | solution.py:757
  66.1 0.7 copy.19
  66.8 0.6 copy.20
